TPU v7x, 1024 devices: a whole 4x8x16 slice. The times are simulated.
1024 devices in a mesh: sp: 256 (over z, y, core), tp: 4 (over x).
Axes of the slice: x: 4, y: 8, z: 16, core: 2. Of those that a mesh axis runs over, the one named last changes fastest.
Arguments:
- tokens: bfloat16 [65536, 2048], P('sp'), may hold values from -28 to 28
- query_weight: bfloat16 [2048, 1536], P(None, 'tp'), may hold values from -0.125 to 0.125
- key_weight: bfloat16 [2048, 1536], P(None, 'tp'), may hold values from -0.125 to 0.125
- value_weight: bfloat16 [2048, 1536], P(None, 'tp'), may hold values from -0.125 to 0.125
- out_weight: bfloat16 [512, 2048], P(None, 'tp'), may hold values from -1 to 1
Outputs:
- mixed: bfloat16 [65536, 2048], P('sp', 'tp')
- total_log: float32 [4, 65536], P('tp', 'sp')
All inputs are finite; a program needn't handle non-finite values.
Results may differ from a plain program's by a relative error of at most 0.012.
The roundings to bfloat16 on the way count: a program that leaves them out, or rounds other values in their place, can miss the bound.
Values may be sent and summed in bfloat16 or wider, within the bound.
No kernel may reach another device: no remote copies, remote signals or barrier semaphores. Data moves between devices by JAX's collectives and lax.ppermute only.
A program may use at most 64 MiB of HBM per device.

v0:
```python
import jax
import jax.numpy as jnp
from jax import lax
from jax.sharding import PartitionSpec as P

HEADS = 4
HEAD_DIM = 128
NEAR_WINDOW = 128
MIDDLE_WINDOW = 512
MIDDLE_DILATION = 4
FAR_WINDOW = 2048
FAR_DILATION = 16


def from_behind(block, axis, distance):
    devices = range(lax.axis_size(axis))
    route = [(i - distance, i) for i in devices if i - distance in devices]
    return lax.ppermute(block, axis, route)


def laid_out(pieces, dim):
    dims = list(pieces.shape[1:])
    dims[dim] *= pieces.shape[0]
    return jnp.moveaxis(pieces, 0, dim).reshape(dims)


def sent_to_all(shard, axis):
    copies = jnp.broadcast_to(shard, (lax.axis_size(axis), *shard.shape))
    return lax.all_to_all(copies, axis, split_axis=0, concat_axis=0, tiled=True)


def gather_directly(shard, axis, dim):
    return laid_out(sent_to_all(shard, axis), dim)


def window_table():
    return ((NEAR_WINDOW, 1), (MIDDLE_WINDOW, MIDDLE_DILATION), (FAR_WINDOW, FAR_DILATION))


def tail_counts(row_count, distance, held_rows):
    counts = []
    for entry, available in zip(window_table(), held_rows):
        counts.append(max(0, min(available, entry[0] - (distance - 1) * row_count)))
    return counts


def pack_tails(sources, counts):
    selected = [
        source[:, source.shape[1] - amount :]
        for source, amount in zip(sources, counts)
        if amount > 0
    ]
    return jnp.concatenate(selected, axis=1)


def unpack_rows(packed, counts):
    result = []
    cursor = 0
    for amount in counts:
        result.append(packed[:, cursor : cursor + amount])
        cursor = cursor + amount
    return result


def attend_group(group_queries, buffer, window, dilation, first_key, slopes_here):
    row_count = group_queries.shape[0]
    head_count = group_queries.shape[1]
    head_size = group_queries.shape[2]
    query_split = group_queries.reshape(row_count // dilation, dilation, head_count, head_size)
    key_split = buffer[0].reshape(-1, dilation, head_count, head_size)
    value_split = buffer[1].reshape(-1, dilation, head_count, head_size)
    scores = jnp.einsum(
        "mrhe,nrhe->rhmn", query_split, key_split, preferred_element_type=jnp.float32
    ) * head_size ** (-0.5)
    grid_shape = (row_count // dilation, key_split.shape[0])
    query_slot = lax.broadcasted_iota(jnp.int32, grid_shape, 0)
    key_slot = lax.broadcasted_iota(jnp.int32, grid_shape, 1)
    spacing = query_slot + window // dilation - key_slot
    residue = lax.broadcasted_iota(jnp.int32, (dilation, 1, 1), 0)
    key_place = first_key + residue + dilation * key_slot[None]
    valid = (spacing[None] >= 0) & (spacing[None] <= window // dilation) & (key_place >= 0)
    scores = (
        scores
        - slopes_here[None, :, None, None] * (dilation * spacing).astype(jnp.float32)[None, None]
    )
    masked = jnp.where(valid[:, None], scores, -jnp.inf)
    highest = jnp.max(masked, axis=-1, keepdims=True)
    log_sum = highest + jnp.log(jnp.sum(jnp.exp(masked - highest), axis=-1, keepdims=True))
    probs = jnp.exp(masked - log_sum).astype(jnp.bfloat16)
    attended = jnp.einsum("rhmn,nrhe->mrhe", probs, value_split, preferred_element_type=jnp.float32)
    attended = attended.reshape(row_count, head_count, head_size)
    log_rows = jnp.transpose(log_sum[..., 0], (1, 2, 0)).reshape(head_count, row_count)
    return (attended, log_rows)


def local(tokens, query_weight, key_weight, value_weight, out_weight):
    rows_here = tokens.shape[0]
    local_heads = query_weight.shape[1] // (3 * HEAD_DIM)

    def project(weight_matrix):
        product = jnp.dot(tokens, weight_matrix, preferred_element_type=jnp.float32)
        return product.astype(jnp.bfloat16).reshape(rows_here, local_heads, 3, HEAD_DIM)

    queries = project(query_weight)
    keys_all = project(key_weight)
    values_all = project(value_weight)
    table = window_table()
    own = [jnp.stack((keys_all[:, :, index], values_all[:, :, index])) for index in range(3)]
    full_rows = [rows_here, rows_here, rows_here]
    reach = -(-FAR_WINDOW // rows_here)
    received = [[], [], []]
    for distance in range(1, reach + 1):
        counts = tail_counts(rows_here, distance, full_rows)
        packed = pack_tails(own, counts)
        arrived = from_behind(packed, "sp", distance)
        for index, rows_block in enumerate(unpack_rows(arrived, counts)):
            if counts[index] > 0:
                received[index].insert(0, rows_block)
    priors = [jnp.concatenate(held_list, axis=1) for held_list in received]
    position_start = lax.axis_index("sp") * rows_here
    head_ids = (
        lax.axis_index("tp") * local_heads + jnp.arange(local_heads, dtype=jnp.int32)
    ).astype(jnp.float32)
    outputs = []
    logs = []
    for index, (window, dilation) in enumerate(table):
        buffer = jnp.concatenate((priors[index], own[index]), axis=1)
        slopes_here = 2.0 ** (3.0 - 8.0 * (head_ids + 1.0) / HEADS) / window
        attended, log_rows = attend_group(
            queries[:, :, index], buffer, window, dilation, position_start - window, slopes_here
        )
        outputs.append(attended)
        logs.append(log_rows)
    stacked_logs = jnp.stack(logs)
    highest = jnp.max(stacked_logs, axis=0)
    total_log = highest + jnp.log(jnp.sum(jnp.exp(stacked_logs - highest), axis=0))
    mixing = jnp.exp(stacked_logs - total_log)
    merged = outputs[0] * jnp.transpose(mixing[0])[:, :, None]
    merged = merged + outputs[1] * jnp.transpose(mixing[1])[:, :, None]
    merged = merged + outputs[2] * jnp.transpose(mixing[2])[:, :, None]
    merged = merged.astype(jnp.bfloat16).reshape(rows_here, local_heads * HEAD_DIM)
    mixed = jnp.dot(
        gather_directly(merged, "tp", 1), out_weight, preferred_element_type=jnp.float32
    ).astype(jnp.bfloat16)
    return (mixed, total_log)


def solution(mesh):
    return jax.shard_map(
        local,
        mesh=mesh,
        in_specs=(P("sp", None), P(None, "tp"), P(None, "tp"), P(None, "tp"), P(None, "tp")),
        out_specs=(P("sp", "tp"), P("tp", "sp")),
        check_vma=False,
    )
```

profile of v0, /device:TPU:304, one launch (start us, length us, event | category | flops | bytes accessed | tf_op | source)
XLA Modules:
  0.0 101.8 jit_solution(16073766818855619241)
XLA Ops:
  0.7 1.4 %copy-done = bf16[2048,384]{1,0:T(8,128)(2,1)S(1)} copy-done((bf16[2048,384]{1,0:T(8,128)(2,1)S(1)}, bf16[2048,384]{1,0:T(8,128)(2,1)}, u32[]{:S(2)}) %copy-start) | copy-done | bytes 1572888
  2.0 1.9 %convolution_convert_fusion.3 = bf16[256,384]{1,0:T(8,128)(2,1)S(1)} fusion(bf16[256,2048]{1,0:T(8,128)(2,1)} %param.5, bf16[2048,384]{1,0:T(8,128)(2,1)S(1)} %copy-done), kind=kOutput, calls=%fused_computation.6 | convolution fusion | flops 402751488 | bytes 2818048 | tf_op jit(solution)/shard_map/dot_general | solution.py:101
  4.0 0.1 copy.70
  4.1 2.1 %convolution_convert_fusion.2 = bf16[256,384]{1,0:T(8,128)(2,1)S(1)} fusion(bf16[256,2048]{1,0:T(8,128)(2,1)S(1)} %copy-done.16, bf16[2048,384]{1,0:T(8,128)(2,1)} %param.8), kind=kOutput, calls=%fused_computation.5 | convolution fusion | flops 402751488 | bytes 2818048 | tf_op jit(solution)/shard_map/dot_general | solution.py:101
  6.3 0.1 copy.71
  6.4 0.7 pad_maximum_fusion.1
  7.1 5.6 %collective-permute-start.2 = (bf16[2,256,1,128]{1,3,2,0:T(8,128)(2,1)}, bf16[2,256,1,128]{1,3,2,0:T(8,128)(2,1)S(1)}, u32[]{:S(2)}, u32[]{:S(2)}) collective-permute-start(bf16[2,256,1,128]{1,3,2,0:T(8,128)(2,1)} %pad_maximum_fusion.1), channel_id=1, source_target_pairs={{0,32},{4,36},{8,40},{12,44},{16,48},{20,52},{24,56},{28,60},{32,6... | collective-permute-start | bytes 393224 | tf_op jit(solution)/shard_map/ppermute | solution.py:18
  12.7 5.0 %collective-permute-start.3 = (bf16[2,256,1,128]{1,3,2,0:T(8,128)(2,1)}, bf16[2,256,1,128]{1,3,2,0:T(8,128)(2,1)S(1)}, u32[]{:S(2)}, u32[]{:S(2)}) collective-permute-start(bf16[2,256,1,128]{1,3,2,0:T(8,128)(2,1)} %pad_maximum_fusion.1), channel_id=1, source_target_pairs={{0,28},{4,32},{8,36},{12,40},{16,44},{20,48},{24,52},{28,56},{32,6... | collective-permute-start | bytes 393224 | tf_op jit(solution)/shard_map/ppermute | solution.py:18
  17.7 3.7 %collective-permute-start.4 = (bf16[2,256,1,128]{1,3,2,0:T(8,128)(2,1)}, bf16[2,256,1,128]{1,3,2,0:T(8,128)(2,1)}, u32[]{:S(2)}, u32[]{:S(2)}) collective-permute-start(bf16[2,256,1,128]{1,3,2,0:T(8,128)(2,1)} %pad_maximum_fusion.1), channel_id=1, source_target_pairs={{0,24},{4,28},{8,32},{12,36},{16,40},{20,44},{24,48},{28,52},{32,5... | collective-permute-start | bytes 393224 | tf_op jit(solution)/shard_map/ppermute | solution.py:18
  21.4 5.8 %collective-permute-start.5 = (bf16[2,256,1,128]{1,3,2,0:T(8,128)(2,1)}, bf16[2,256,1,128]{1,3,2,0:T(8,128)(2,1)}, u32[]{:S(2)}, u32[]{:S(2)}) collective-permute-start(bf16[2,256,1,128]{1,3,2,0:T(8,128)(2,1)} %pad_maximum_fusion.1), channel_id=1, source_target_pairs={{0,20},{4,24},{8,28},{12,32},{16,36},{20,40},{24,44},{28,48},{32,5... | collective-permute-start | bytes 393224 | tf_op jit(solution)/shard_map/ppermute | solution.py:18
  27.2 4.8 %collective-permute-start.6 = (bf16[2,256,1,128]{1,3,2,0:T(8,128)(2,1)}, bf16[2,256,1,128]{1,3,2,0:T(8,128)(2,1)}, u32[]{:S(2)}, u32[]{:S(2)}) collective-permute-start(bf16[2,256,1,128]{1,3,2,0:T(8,128)(2,1)} %pad_maximum_fusion.1), channel_id=1, source_target_pairs={{0,16},{4,20},{8,24},{12,28},{16,32},{20,36},{24,40},{28,44},{32,4... | collective-permute-start | bytes 393224 | tf_op jit(solution)/shard_map/ppermute | solution.py:18
  32.1 0.6 iota_add_fusion
  32.7 0.7 fusion.29
  33.4 0.7 convert_multiply_fusion
  34.1 2.4 %convolution_convert_fusion.1 = bf16[256,384]{1,0:T(8,128)(2,1)S(1)} fusion(bf16[256,2048]{1,0:T(8,128)(2,1)} %param.5, bf16[2048,384]{1,0:T(8,128)(2,1)} %param.6), kind=kOutput, calls=%fused_computation.4 | convolution fusion | flops 402751488 | bytes 2818048 | tf_op jit(solution)/shard_map/dot_general | solution.py:101
  36.6 0.1 copy.74
  36.7 0.7 fusion.32
  37.4 0.7 convert_multiply_fusion.1
  38.1 0.6 iota_add_fusion.3
  38.7 0.5 iota_add_fusion.1
  39.2 0.7 copy.76
  40.0 0.7 copy.81
  40.7 1.9 %collective-permute-start.7 = (bf16[2,256,1,128]{1,3,2,0:T(8,128)(2,1)}, bf16[2,256,1,128]{1,3,2,0:T(8,128)(2,1)S(1)}, u32[]{:S(2)}, u32[]{:S(2)}) collective-permute-start(bf16[2,256,1,128]{1,3,2,0:T(8,128)(2,1)} %pad_maximum_fusion.1), channel_id=1, source_target_pairs={{0,12},{4,16},{8,20},{12,24},{16,28},{20,32},{24,36},{28,40},{32,4... | collective-permute-start | bytes 393224 | tf_op jit(solution)/shard_map/ppermute | solution.py:18
  42.6 0.7 constant_dynamic-update-slice_fusion.6
  43.3 2.6 %collective-permute-start.1 = (bf16[2,512,1,128]{1,3,2,0:T(8,128)(2,1)S(1)}, bf16[2,512,1,128]{1,3,2,0:T(8,128)(2,1)S(1)}, u32[]{:S(2)}, u32[]{:S(2)}) collective-permute-start(bf16[2,512,1,128]{1,3,2,0:T(8,128)(2,1)S(1)} %maximum_maximum_fusion.1), channel_id=1, source_target_pairs={{0,8},{4,12},{8,16},{12,20},{16,24},{20,28},{24,32},{28,36},{32,40... | collective-permute-start | bytes 786440 | tf_op jit(solution)/shard_map/ppermute | solution.py:18
  45.9 0.7 constant_dynamic-update-slice_fusion.5
  46.6 3.4 %collective-permute-start = (bf16[2,640,1,128]{1,3,2,0:T(8,128)(2,1)S(1)}, bf16[2,640,1,128]{1,3,2,0:T(8,128)(2,1)S(1)}, u32[]{:S(2)}, u32[]{:S(2)}) collective-permute-start(bf16[2,640,1,128]{1,3,2,0:T(8,128)(2,1)S(1)} %fusion.17), channel_id=1, source_target_pairs={{0,4},{4,8},{8,12},{12,16},{16,20},{20,24},{24,28},{28,32},{32,36}... | collective-permute-start | bytes 983048 | tf_op jit(solution)/shard_map/ppermute | solution.py:18
  50.0 1.6 %constant_dynamic-update-slice_fusion.4 = bf16[2,2304,1,128]{1,3,2,0:T(8,128)(2,1)} fusion(bf16[2,2304,1,128]{1,3,2,0:T(8,128)(2,1)} %constant_dynamic-update-slice_fusion.5, bf16[2,256,1,128]{1,3,2,0:T(8,128)(2,1)} %collective-permute-done.4), kind=kLoop, calls=%fused_computation.73 | loop fusion | bytes 262144
  51.6 1.6 %constant_dynamic-update-slice_fusion.3 = bf16[2,2304,1,128]{1,3,2,0:T(8,128)(2,1)} fusion(bf16[2,2304,1,128]{1,3,2,0:T(8,128)(2,1)} %constant_dynamic-update-slice_fusion.4, bf16[2,256,1,128]{1,3,2,0:T(8,128)(2,1)} %collective-permute-done.5), kind=kLoop, calls=%fused_computation.72 | loop fusion | bytes 262144
  53.2 3.0 %collective-permute-done.6 = bf16[2,256,1,128]{1,3,2,0:T(8,128)(2,1)} collective-permute-done((bf16[2,256,1,128]{1,3,2,0:T(8,128)(2,1)}, bf16[2,256,1,128]{1,3,2,0:T(8,128)(2,1)}, u32[]{:S(2)}, u32[]{:S(2)}) %collective-permute-start.6) | collective-permute-done | bytes 131104 | tf_op jit(solution)/shard_map/ppermute | solution.py:18
  56.2 1.6 %constant_dynamic-update-slice_fusion.2 = bf16[2,2304,1,128]{1,3,2,0:T(8,128)(2,1)} fusion(bf16[2,2304,1,128]{1,3,2,0:T(8,128)(2,1)} %constant_dynamic-update-slice_fusion.3, bf16[2,256,1,128]{1,3,2,0:T(8,128)(2,1)} %collective-permute-done.6), kind=kLoop, calls=%fused_computation.71 | loop fusion | bytes 262144
  57.7 0.1 collective-permute-done.7
  57.9 0.7 constant_dynamic-update-slice_fusion.1
  58.6 11.6 %collective-permute-done.1 = bf16[2,512,1,128]{1,3,2,0:T(8,128)(2,1)S(1)} collective-permute-done((bf16[2,512,1,128]{1,3,2,0:T(8,128)(2,1)S(1)}, bf16[2,512,1,128]{1,3,2,0:T(8,128)(2,1)S(1)}, u32[]{:S(2)}, u32[]{:S(2)}) %collective-permute-start.1) | collective-permute-done | bytes 262176 | tf_op jit(solution)/shard_map/ppermute | solution.py:18
  70.2 0.7 fusion.36
  70.9 1.5 %collective-permute-done = bf16[2,640,1,128]{1,3,2,0:T(8,128)(2,1)S(1)} collective-permute-done((bf16[2,640,1,128]{1,3,2,0:T(8,128)(2,1)S(1)}, bf16[2,640,1,128]{1,3,2,0:T(8,128)(2,1)S(1)}, u32[]{:S(2)}, u32[]{:S(2)}) %collective-permute-start) | collective-permute-done | bytes 327712 | tf_op jit(solution)/shard_map/ppermute | solution.py:18
  72.4 0.7 fusion.35
  73.2 0.2 copy.77
  73.4 0.3 fusion.41
  73.8 0.2 exponential_reduce_fusion.2
  74.1 0.7 stack.29
  74.7 0.7 stack.26
  75.4 0.7 constant_dynamic-update-slice_fusion
  76.1 1.3 %fusion.33 = (bf16[1,2304,1,128]{1,3,2,0:T(8,128)(2,1)S(1)}, bf16[1,2304,1,128]{1,3,2,0:T(8,128)(2,1)S(1)}) fusion(bf16[2,2304,1,128]{1,3,2,0:T(8,128)(2,1)} %constant_dynamic-update-slice_fusion), kind=kLoop, calls=%fused_computation.96 | loop fusion | bytes 2359296 | tf_op jit(solution)/shard_map/slice | solution.py:71
  77.5 1.1 %copy.82 = bf16[1,2304,1,128]{3,1,2,0:T(8,128)(2,1)} copy(bf16[1,2304,1,128]{1,3,2,0:T(8,128)(2,1)S(1)} %get-tuple-element.7) | data formatting | bytes 1179648 | tf_op jit(solution)/shard_map/slice | solution.py:70
  78.5 1.6 %fusion.40 = (f32[16,16]{1,0:T(8,128)S(1)}, f32[16,16,144]{2,1,0:T(8,128)S(1)}) fusion(f32[16,144]{1,0:T(8,128)} %convert_multiply_fusion.1, bf16[144,16,128]{2,1,0:T(8,128)(2,1)} %bitcast.87, bf16[16,16,128]{2,1,0:T(8,128)(2,1)S(1)} %bitcast.94, s32[16,144]{1,0:T(8,128)S(1)} %iota_multiply_fusion.1, s32[16]{0:T(128)S(1)} %copy-done.18, ...), kind=kOutput, calls=%fused_computation.103 | convolution fusion | flops 9694976 | bytes 824640 | tf_op jit(solution)/shard_map/mrhe,nrhe->rhmn/dot_general | solution.py:72
  80.1 0.7 copy-done.1
  80.8 0.2 exponential_reduce_fusion.1
  81.3 0.7 reduce_max.82
  82.0 0.7 reduce_max.84
  82.7 1.3 %fusion.42 = (f32[256]{0:T(256)S(1)}, f32[256,384]{1,0:T(8,128)S(1)}) fusion(f32[]{:T(128)S(6)} %div.18, bf16[2,384,1,128]{1,3,2,0:T(8,128)(2,1)S(1)} %maximum_maximum_fusion.2, bf16[256,1,3,128]{0,3,2,1:T(8,128)(2,1)} %bitcast.89, s32[]{:T(128)S(6)} %sub.159, s32[256]{0:T(256)S(1)} %copy-done.17), kind=kOutput, calls=%fused_computation.105 | convolution fusion | flops 26443520 | bytes 559112 | tf_op jit(solution)/shard_map/mrhe,nrhe->rhmn/dot_general | solution.py:72
  84.0 0.2 exponential_reduce_fusion
  84.3 0.6 fusion.39
  84.8 0.6 fusion.38
  85.4 0.2 copy.88
  85.6 0.2 convolution_bitcast_fusion.1
  86.1 0.3 copy.92
  86.4 1.3 %convolution_bitcast_fusion = f32[16,16,1,128]{3,0,1,2:T(8,128)S(1)} fusion(bf16[144,16,128]{2,1,0:T(8,128)(2,1)S(1)} %bitcast.82, f32[16,16,144]{2,1,0:T(8,128)} %copy-done.1, f32[16,16]{1,0:T(8,128)S(1)} %log_add_fusion), kind=kOutput, calls=%fused_computation.13 | convolution fusion | flops 9510912 | bytes 869376 | tf_op jit(solution)/shard_map/rhmn,nrhe->mrhe/dot_general | solution.py:90
  87.8 1.2 %fusion.9 = bf16[256,128]{0,1:T(8,128)(2,1)S(1)} fusion(f32[256,384]{1,0:T(8,128)S(1)} %get-tuple-element.32, f32[256]{0:T(256)S(1)} %get-tuple-element.5, f32[256,128]{0,1:T(8,128)S(1)} %copy.95, f32[256,128]{0,1:T(8,128)S(1)} %copy.91, bf16[2,384,1,128]{1,3,2,0:T(8,128)(2,1)} %copy-done.4, f32[256]{0:T(256)} %bitcast.100, f32[256]{0:T(256)} %bitcast.101, ...), kind=kOutput, calls=%fused_computation.19 | convolution fusion | flops 25559040 | bytes 823296 | tf_op jit(solution)/shard_map/rhmn,nrhe->mrhe/dot_general | solution.py:90
  89.1 0.7 broadcast_in_dim.15
  89.8 4.3 %all-to-all-start = ((bf16[4,256,128]{1,2,0:T(8,128)(2,1)}), bf16[4,256,128]{1,2,0:T(8,128)(2,1)S(1)}, u32[]{:S(2)}, u32[]{:S(2)}) async-start(bf16[4,256,128]{1,2,0:T(8,128)(2,1)} %broadcast_in_dim.15), calls=%async_computation | async-start | bytes 524288 | tf_op jit(solution)/shard_map/all_to_all | solution.py:29
  94.1 0.6 maximum_add_fusion
  94.6 6.1 %all-to-all-done = bf16[4,256,128]{1,2,0:T(8,128)(2,1)S(1)} async-done(((bf16[4,256,128]{1,2,0:T(8,128)(2,1)}), bf16[4,256,128]{1,2,0:T(8,128)(2,1)S(1)}, u32[]{:S(2)}, u32[]{:S(2)}) %all-to-all-start) | async-done | bytes 262176 | tf_op jit(solution)/shard_map/all_to_all | solution.py:29
  100.7 1.0 %convolution_convert_fusion = bf16[256,512]{1,0:T(8,128)(2,1)} fusion(bf16[256,512]{0,1:T(8,128)(2,1)S(1)} %bitcast.83, bf16[512,512]{1,0:T(8,128)(2,1)S(1)} %copy-done.3), kind=kOutput, calls=%fused_computation | convolution fusion | flops 134348800 | bytes 1048576 | tf_op jit(solution)/shard_map/dot_general | solution.py:142
  (68 shorter events, 1.0 us)
Async XLA Ops:
  0.6 1.4 %copy-start = (bf16[2048,384]{1,0:T(8,128)(2,1)S(1)}, bf16[2048,384]{1,0:T(8,128)(2,1)}, u32[]{:S(2)}) copy-start(bf16[2048,384]{1,0:T(8,128)(2,1)} %param.7) | copy-start | bytes 4718596
  0.6 3.5 %copy-start.16 = (bf16[256,2048]{1,0:T(8,128)(2,1)S(1)}, bf16[256,2048]{1,0:T(8,128)(2,1)}, u32[]{:S(2)}) copy-start(bf16[256,2048]{1,0:T(8,128)(2,1)} %param.5) | copy-start | bytes 3145732
  7.1 33.6 %collective-permute-start.2 = (bf16[2,256,1,128]{1,3,2,0:T(8,128)(2,1)}, bf16[2,256,1,128]{1,3,2,0:T(8,128)(2,1)S(1)}, u32[]{:S(2)}, u32[]{:S(2)}) collective-permute-start(bf16[2,256,1,128]{1,3,2,0:T(8,128)(2,1)} %pad_maximum_fusion.1), channel_id=1, source_target_pairs={{0,32},{4,36},{8,40},{12,44},{16,48},{20,52},{24,56},{28,60},{32,6... | collective-permute-start | bytes 393224 | tf_op jit(solution)/shard_map/ppermute | solution.py:18
  12.7 30.6 %collective-permute-start.3 = (bf16[2,256,1,128]{1,3,2,0:T(8,128)(2,1)}, bf16[2,256,1,128]{1,3,2,0:T(8,128)(2,1)S(1)}, u32[]{:S(2)}, u32[]{:S(2)}) collective-permute-start(bf16[2,256,1,128]{1,3,2,0:T(8,128)(2,1)} %pad_maximum_fusion.1), channel_id=1, source_target_pairs={{0,28},{4,32},{8,36},{12,40},{16,44},{20,48},{24,52},{28,56},{32,6... | collective-permute-start | bytes 393224 | tf_op jit(solution)/shard_map/ppermute | solution.py:18
  17.7 28.8 %collective-permute-start.4 = (bf16[2,256,1,128]{1,3,2,0:T(8,128)(2,1)}, bf16[2,256,1,128]{1,3,2,0:T(8,128)(2,1)}, u32[]{:S(2)}, u32[]{:S(2)}) collective-permute-start(bf16[2,256,1,128]{1,3,2,0:T(8,128)(2,1)} %pad_maximum_fusion.1), channel_id=1, source_target_pairs={{0,24},{4,28},{8,32},{12,36},{16,40},{20,44},{24,48},{28,52},{32,5... | collective-permute-start | bytes 393224 | tf_op jit(solution)/shard_map/ppermute | solution.py:18
  21.4 30.2 %collective-permute-start.5 = (bf16[2,256,1,128]{1,3,2,0:T(8,128)(2,1)}, bf16[2,256,1,128]{1,3,2,0:T(8,128)(2,1)}, u32[]{:S(2)}, u32[]{:S(2)}) collective-permute-start(bf16[2,256,1,128]{1,3,2,0:T(8,128)(2,1)} %pad_maximum_fusion.1), channel_id=1, source_target_pairs={{0,20},{4,24},{8,28},{12,32},{16,36},{20,40},{24,44},{28,48},{32,5... | collective-permute-start | bytes 393224 | tf_op jit(solution)/shard_map/ppermute | solution.py:18
  27.2 28.9 %collective-permute-start.6 = (bf16[2,256,1,128]{1,3,2,0:T(8,128)(2,1)}, bf16[2,256,1,128]{1,3,2,0:T(8,128)(2,1)}, u32[]{:S(2)}, u32[]{:S(2)}) collective-permute-start(bf16[2,256,1,128]{1,3,2,0:T(8,128)(2,1)} %pad_maximum_fusion.1), channel_id=1, source_target_pairs={{0,16},{4,20},{8,24},{12,28},{16,32},{20,36},{24,40},{28,44},{32,4... | collective-permute-start | bytes 393224 | tf_op jit(solution)/shard_map/ppermute | solution.py:18
  36.7 14.9 %copy-start.2 = (bf16[256,384]{0,1:T(8,128)(2,1)}, bf16[256,384]{0,1:T(8,128)(2,1)S(1)}, u32[]{:S(2)}) copy-start(bf16[256,384]{0,1:T(8,128)(2,1)S(1)} %copy.74) | copy-start | bytes 589828
  40.7 17.2 %collective-permute-start.7 = (bf16[2,256,1,128]{1,3,2,0:T(8,128)(2,1)}, bf16[2,256,1,128]{1,3,2,0:T(8,128)(2,1)S(1)}, u32[]{:S(2)}, u32[]{:S(2)}) collective-permute-start(bf16[2,256,1,128]{1,3,2,0:T(8,128)(2,1)} %pad_maximum_fusion.1), channel_id=1, source_target_pairs={{0,12},{4,16},{8,20},{12,24},{16,28},{20,32},{24,36},{28,40},{32,4... | collective-permute-start | bytes 393224 | tf_op jit(solution)/shard_map/ppermute | solution.py:18
  43.3 26.9 %collective-permute-start.1 = (bf16[2,512,1,128]{1,3,2,0:T(8,128)(2,1)S(1)}, bf16[2,512,1,128]{1,3,2,0:T(8,128)(2,1)S(1)}, u32[]{:S(2)}, u32[]{:S(2)}) collective-permute-start(bf16[2,512,1,128]{1,3,2,0:T(8,128)(2,1)S(1)} %maximum_maximum_fusion.1), channel_id=1, source_target_pairs={{0,8},{4,12},{8,16},{12,20},{16,24},{20,28},{24,32},{28,36},{32,40... | collective-permute-start | bytes 786440 | tf_op jit(solution)/shard_map/ppermute | solution.py:18
  46.6 25.9 %collective-permute-start = (bf16[2,640,1,128]{1,3,2,0:T(8,128)(2,1)S(1)}, bf16[2,640,1,128]{1,3,2,0:T(8,128)(2,1)S(1)}, u32[]{:S(2)}, u32[]{:S(2)}) collective-permute-start(bf16[2,640,1,128]{1,3,2,0:T(8,128)(2,1)S(1)} %fusion.17), channel_id=1, source_target_pairs={{0,4},{4,8},{8,12},{12,16},{16,20},{20,24},{24,28},{28,32},{32,36}... | collective-permute-start | bytes 983048 | tf_op jit(solution)/shard_map/ppermute | solution.py:18
  72.4 3.0 %copy-start.5 = (bf16[2,640,1,128]{1,3,2,0:T(8,128)(2,1)}, bf16[2,640,1,128]{1,3,2,0:T(8,128)(2,1)S(1)}, u32[]{:S(2)}) copy-start(bf16[2,640,1,128]{1,3,2,0:T(8,128)(2,1)S(1)} %collective-permute-done) | copy-start | bytes 983044
  72.4 1.0 copy-start.6
  72.4 1.0 copy-start.8
  72.4 1.0 copy-start.9
  72.4 1.0 copy-start.19
  77.4 1.1 %copy-start.7 = (bf16[256,1,1,128]{3,0,2,1:T(8,128)(2,1)S(1)}, bf16[256,1,1,128]{3,0,2,1:T(8,128)(2,1)}, u32[]{:S(2)}) copy-start(bf16[256,1,1,128]{3,0,2,1:T(8,128)(2,1)} %copy.81) | copy-start | bytes 196612
  77.4 1.1 %copy-start.12 = (pred[16,144]{1,0:T(8,128)(4,1)S(1)}, pred[16,144]{1,0:T(8,128)(4,1)}, u32[]{:S(2)}) copy-start(pred[16,144]{1,0:T(8,128)(4,1)} %fusion.32) | copy-start | bytes 6916
  77.4 1.1 %copy-start.18 = (s32[16]{0:T(128)S(1)}, s32[16]{0:T(128)}, u32[]{:S(2)}) copy-start(s32[16]{0:T(128)} %iota_add_fusion.1) | copy-start | bytes 196
  77.5 5.2 %slice-start = ((bf16[2,640,1,128]{1,3,2,0:T(8,128)(2,1)}), bf16[2,128,1,128]{1,3,2,0:T(8,128)(2,1)S(1)}, s32[]{:S(2)}) async-start(bf16[2,640,1,128]{1,3,2,0:T(8,128)(2,1)} %copy-done.5), calls=%async_computation.1 | async-start | bytes 131072 | tf_op jit(solution)/shard_map/slice | solution.py:60
  78.5 4.1 %copy-start.17 = (s32[256]{0:T(256)S(1)}, s32[256]{0:T(256)}, u32[]{:S(2)}) copy-start(s32[256]{0:T(256)} %iota_add_fusion) | copy-start | bytes 3076
  80.1 0.7 copy-start.1
  82.0 2.2 %copy-start.14 = (f32[256]{0:T(256)S(1)}, f32[256]{0:T(256)}, u32[]{:S(2)}) copy-start(f32[256]{0:T(256)} %stack.29) | copy-start | bytes 3076
  82.6 1.6 %copy-start.15 = (f32[1,1,256]{2,1,0:T(1,128)S(1)}, f32[1,1,256]{2,1,0:T(1,128)}, u32[]{:S(2)}) copy-start(f32[1,1,256]{2,1,0:T(1,128)} %stack.26) | copy-start | bytes 3076
  82.7 2.8 %copy-start.4 = (bf16[2,384,1,128]{1,3,2,0:T(8,128)(2,1)}, bf16[2,384,1,128]{1,3,2,0:T(8,128)(2,1)S(1)}, u32[]{:S(2)}) copy-start(bf16[2,384,1,128]{1,3,2,0:T(8,128)(2,1)S(1)} %maximum_maximum_fusion.2) | copy-start | bytes 589828
  87.6 6.4 %copy-start.10 = (f32[1,256]{1,0:T(1,128)S(1)}, f32[1,256]{1,0:T(1,128)}, u32[]{:S(2)}) copy-start(f32[1,256]{1,0:T(1,128)} %reduce_max.82) | copy-start | bytes 3076
  87.6 6.4 %copy-start.11 = (f32[1,256]{1,0:T(1,128)S(1)}, f32[1,256]{1,0:T(1,128)}, u32[]{:S(2)}) copy-start(f32[1,256]{1,0:T(1,128)} %reduce_max.84) | copy-start | bytes 3076
  87.6 6.4 %copy-start.13 = (f32[256]{0:T(256)S(1)}, f32[256]{0:T(256)}, u32[]{:S(2)}) copy-start(f32[256]{0:T(256)} %get-tuple-element.25) | copy-start | bytes 3076
  87.6 13.1 %copy-start.3 = (bf16[512,512]{1,0:T(8,128)(2,1)S(1)}, bf16[512,512]{1,0:T(8,128)(2,1)}, u32[]{:S(2)}) copy-start(bf16[512,512]{1,0:T(8,128)(2,1)} %param.9) | copy-start | bytes 1572868
  89.8 11.0 %all-to-all-start = ((bf16[4,256,128]{1,2,0:T(8,128)(2,1)}), bf16[4,256,128]{1,2,0:T(8,128)(2,1)S(1)}, u32[]{:S(2)}, u32[]{:S(2)}) async-start(bf16[4,256,128]{1,2,0:T(8,128)(2,1)} %broadcast_in_dim.15), calls=%async_computation | async-start | bytes 524288 | tf_op jit(solution)/shard_map/all_to_all | solution.py:29
where the time goes:
time: 103 us; the launch traced here: 102 us
  starting transfers between devices  37.1 us (36%)
  waiting for transfers between devices  22.4 us (22%)
  local copies, waits for them, and re-layouts  20.1 us (20%)
  matrix products  13.5 us (13%)
  other arithmetic  7.66 us (7%)
  between operations  1.12 us (1%)
    ppermute x8, starting transfers between devices, from_behind(): return lax.ppermute(block, axis, route)  32.8 us
    ppermute x8, waiting for transfers between devices, from_behind(): return lax.ppermute(block, axis, route)  16.3 us
    unnamed x46, local copies, waits for them, and re-layouts  9.07 us
    dot_general x3, matrix products, project(): product = jnp.dot(tokens, weight_matrix, preferred_element_type=jnp.float32)  6.48 us
    all_to_all x1, waiting for transfers between devices, sent_to_all(): return lax.all_to_all(copies, axis, split_axis=0, concat_axis=0, tiled=True)  6.1 us
    all_to_all x1, starting transfers between devices, sent_to_all(): return lax.all_to_all(copies, axis, split_axis=0, concat_axis=0, tiled=True)  4.29 us
    dot_general x3, matrix products, attend_group(): jnp.einsum('mrhe,nrhe->rhmn', query_split, key_split, preferred_element_t...  3.21 us
    dot_general x3, matrix products, attend_group(): jnp.einsum('rhmn,nrhe->mrhe', probs, value_split, preferred_element_type=...  2.75 us
  transfers between devices with their start and end apart: 9, of which 5 were waited for; matrix products, arithmetic and copies ran while one was open for 16% of the time, Pallas kernels for 0%

commit v1 on v0

v1 whole, which is shorter than its diff:
```python
import jax
import jax.numpy as jnp
from jax import lax
from jax.experimental import pallas as pl
from jax.experimental.pallas import tpu as pltpu
from jax.sharding import Mesh
from jax.sharding import PartitionSpec as P

HEAD_DIM = 128
TOK = 256
PLANE = 16
RUN = TOK // PLANE
BAND = 128
MIDDLE_DILATION = 4
SCALE = HEAD_DIM**-0.5
K_STEPS = 4
F32 = jnp.float32
BF16 = jnp.bfloat16
VMEM = pltpu.VMEM
WHOLE = pl.BlockSpec(memory_space=pltpu.VMEM)


def iota(shape, dim):
    return lax.broadcasted_iota(jnp.int32, shape, dim)


def residue_order():
    row, col = iota((TOK, TOK), 0), iota((TOK, TOK), 1)
    return jnp.where(col == (row % RUN) * PLANE + row // RUN, 1.0, 0.0).astype(BF16)


def head_slope():
    head = lax.axis_index("tp")
    return jnp.where(head == 0, 2.0, jnp.where(head == 1, 0.5, jnp.where(head == 2, 0.125, 0.03125)))


def times_transposed(a, b):
    return lax.dot_general(a, b, (((1,), (1,)), ((), ())), preferred_element_type=F32)


def soft(scores, valid, values):
    scores = jnp.where(valid, scores, -jnp.inf)
    highest = jnp.max(scores, axis=1, keepdims=True)
    weights = jnp.exp(scores - highest)
    total = jnp.sum(weights, axis=1, keepdims=True)
    probs = (weights * (1.0 / total)).astype(BF16)
    return jnp.dot(probs, values, preferred_element_type=F32), highest + jnp.log(total)


def banded(queries, keys, values, slope, has_prior):
    shape = (TOK, TOK + BAND)
    spacing = iota(shape, 0) + BAND - iota(shape, 1)
    first = jnp.where(has_prior, 0, BAND)
    valid = (spacing >= 0) & (spacing <= BAND) & (iota(shape, 1) >= first)
    scores = times_transposed(queries, keys) * SCALE - slope * spacing.astype(F32)
    return soft(scores, valid, values)


def project_body(tok, wq, wk, wv, far, queries, near, sent_one, sent_two, acc):
    step = pl.program_id(0)

    @pl.when(step == 0)
    def _():
        acc[...] = jnp.zeros_like(acc)

    x = tok[...]
    for j, w in enumerate((wq, wk, wv)):
        acc[j] += jnp.dot(x, w[...], preferred_element_type=F32)

    @pl.when(step == pl.num_programs(0) - 1)
    def _():
        q, k, v = acc[0].astype(BF16), acc[1].astype(BF16), acc[2].astype(BF16)
        d = HEAD_DIM
        order = residue_order()
        for j, part in enumerate((q, k, v)):
            sorted_rows = jnp.dot(order, part[:, 2 * d :], preferred_element_type=F32).astype(BF16)
            far[:, j * RUN : (j + 1) * RUN] = sorted_rows.reshape(PLANE, RUN, d)
        queries[0] = q[:, :d]
        queries[1] = q[:, d : 2 * d]
        near[0] = k[:BAND, :d]
        near[1] = v[:BAND, :d]
        sent_one[:BAND] = k[BAND:, :d]
        sent_one[BAND : 2 * BAND] = v[BAND:, :d]
        for j, part in enumerate((k, v)):
            rows = part[:, d : 2 * d]
            sent_one[2 * BAND + j * TOK : 2 * BAND + (j + 1) * TOK] = rows
            sent_two[j * TOK : (j + 1) * TOK] = rows


def project(tokens, wq, wk, wv):
    width, cols = wq.shape
    chunk = width // K_STEPS
    d = HEAD_DIM
    weight = pl.BlockSpec((chunk, cols), lambda i: (i, 0))
    return pl.pallas_call(
        project_body,
        grid=(K_STEPS,),
        in_specs=[pl.BlockSpec((TOK, chunk), lambda i: (0, i)), weight, weight, weight],
        out_specs=[WHOLE] * 5,
        out_shape=[
            VMEM((PLANE, 3 * RUN, d), BF16),
            VMEM((2, TOK, d), BF16),
            VMEM((2, BAND, d), BF16),
            VMEM((2 * BAND + 2 * TOK, d), BF16),
            VMEM((2 * TOK, d), BF16),
        ],
        scratch_shapes=[pltpu.VMEM((3, TOK, cols), F32)],
        name="project",
    )(tokens, wq, wk, wv)


def near_middle_body(queries, near, own, one, two, attended, log):
    slope = head_slope()
    place = lax.axis_index("z") * PLANE + lax.axis_index("yc")
    b = BAND
    keys = jnp.concatenate((one[:b], near[0], own[:b]), axis=0)
    values = jnp.concatenate((one[b : 2 * b], near[1], own[b : 2 * b]), axis=0)
    first, first_log = banded(queries[0], keys, values, slope / b, place > 0)

    k_at, v_at = slice(2 * b, 2 * b + TOK), slice(2 * b + TOK, 2 * b + 2 * TOK)
    keys = jnp.concatenate((two[:TOK], one[k_at], own[k_at]), axis=0)
    values = jnp.concatenate((two[TOK:], one[v_at], own[v_at]), axis=0)
    shape = (TOK, 3 * TOK)
    window = MIDDLE_DILATION * BAND
    spacing = iota(shape, 0) + window - iota(shape, 1)
    begin = jnp.maximum(window - place * TOK, 0)
    valid = (spacing >= 0) & (spacing <= window) & (spacing % MIDDLE_DILATION == 0)
    valid = valid & (iota(shape, 1) >= begin)
    scores = times_transposed(queries[1], keys) * SCALE - (slope / window) * spacing.astype(F32)
    second, second_log = soft(scores, valid, values)

    highest = jnp.maximum(first_log, second_log)
    first_share, second_share = jnp.exp(first_log - highest), jnp.exp(second_log - highest)
    total = first_share + second_share
    inverse = 1.0 / total
    attended[...] = (first_share * inverse) * first + (second_share * inverse) * second
    log[...] = jnp.broadcast_to(highest + jnp.log(total), log.shape)


def near_middle(queries, near, own, one, two):
    shape = (TOK, HEAD_DIM)
    return pl.pallas_call(
        near_middle_body,
        in_specs=[WHOLE] * 5,
        out_specs=[WHOLE] * 2,
        out_shape=[VMEM(shape, F32), VMEM(shape, F32)],
        name="near_middle",
    )(queries, near, own, one, two)


def far_body(mine, halo, out):
    d, r = HEAD_DIM, RUN
    slope = head_slope() / BAND
    queries = mine[:, :r].reshape(TOK, d)
    keys = jnp.concatenate((halo[:, :r].reshape(BAND, d), mine[:, r : 2 * r].reshape(TOK, d)), axis=0)
    values = jnp.concatenate((halo[:, r:].reshape(BAND, d), mine[:, 2 * r :].reshape(TOK, d)), axis=0)
    attended, log = banded(queries, keys, values, slope, lax.axis_index("z") > 0)
    out[:, :r] = attended.astype(BF16).reshape(PLANE, r, d)
    lanes = iota((TOK, d), 1)
    slots = iota((TOK, d), 0) % r
    rows = jnp.sum(jnp.where(lanes == slots, log, 0.0).reshape(PLANE, r, d), axis=1)
    high = rows.astype(BF16).astype(F32)
    middle = (rows - high).astype(BF16).astype(F32)
    low = rows - high - middle
    at = iota((PLANE, 8, d), 1)
    parts = jnp.where(at == 0, high[:, None], jnp.where(at == 1, middle[:, None], low[:, None]))
    out[:, r:] = jnp.where(at < 3, parts, 0.0).astype(BF16)


def far_attention(mine, halo):
    return pl.pallas_call(
        far_body,
        in_specs=[WHOLE] * 2,
        out_specs=WHOLE,
        out_shape=VMEM((PLANE, RUN + 8, HEAD_DIM), BF16),
        name="far",
    )(mine, halo)


def merge_body(attended, log, far, merged, total_log):
    d, r = HEAD_DIM, RUN
    rows = far[:, :r].reshape(TOK, d)
    far_rows = jnp.dot(residue_order(), rows, preferred_element_type=F32)
    logs = jnp.sum(far[:, r:].astype(F32), axis=1)
    spread = jnp.broadcast_to(logs[None], (RUN, PLANE, d)).reshape(TOK, d)
    tokens, lanes = iota((TOK, d), 0), iota((TOK, d), 1)
    far_log = jnp.sum(jnp.where(lanes == tokens // PLANE, spread, 0.0), axis=1, keepdims=True)
    other_log = log[:, :1]
    highest = jnp.maximum(other_log, far_log)
    total = highest + jnp.log(jnp.exp(other_log - highest) + jnp.exp(far_log - highest))
    both = jnp.exp(other_log - total) * attended[...] + jnp.exp(far_log - total) * far_rows
    both = both.astype(BF16)
    for j in range(merged.shape[0]):
        merged[j] = both
    for j in range(TOK // d):
        part = jnp.where(lanes == tokens - j * d, total, 0.0)
        total_log[:, j * d : (j + 1) * d] = jnp.sum(part, axis=0, keepdims=True)


def merge(attended, log, far, copies):
    return pl.pallas_call(
        merge_body,
        in_specs=[WHOLE] * 3,
        out_specs=[WHOLE] * 2,
        out_shape=[VMEM((copies, TOK, HEAD_DIM), BF16), jax.ShapeDtypeStruct((1, TOK), F32)],
        name="merge",
    )(attended, log, far)


def mix_body(heads, weight, out):
    rows = jnp.concatenate([heads[j] for j in range(heads.shape[0])], axis=1)
    out[...] = jnp.dot(rows, weight[...], preferred_element_type=F32).astype(BF16)


def mix(heads, weight):
    return pl.pallas_call(
        mix_body,
        in_specs=[WHOLE] * 2,
        out_specs=WHOLE,
        out_shape=jax.ShapeDtypeStruct((TOK, weight.shape[1]), BF16),
        name="mix",
    )(heads, weight)


def swap(blocks, axis):
    return lax.all_to_all(blocks, axis, split_axis=0, concat_axis=0, tiled=True)


def behind(block, axes, distance):
    count = lax.axis_size(axes)
    return lax.ppermute(block, axes, [(i - distance, i) for i in range(distance, count)])


def local(tokens, query_weight, key_weight, value_weight, out_weight):
    sp = ("z", "yc")
    far, queries, near, sent_one, sent_two = project(tokens, query_weight, key_weight, value_weight)
    mine = swap(far, "yc")
    one, two = behind(sent_one, sp, 1), behind(sent_two, sp, 2)
    halo = behind(mine[PLANE // 2 :, RUN:], "z", 1)
    attended, log = near_middle(queries, near, sent_one, one, two)
    far_out = swap(far_attention(mine, halo), "yc")
    merged, total_log = merge(attended, log, far_out, lax.axis_size("tp"))
    return mix(swap(merged, "tp"), out_weight), total_log


def solution(mesh):
    devices = mesh.devices
    planes = Mesh(devices.reshape(devices.shape[0] // PLANE, PLANE, devices.shape[1]), ("z", "yc", "tp"))
    sp = ("z", "yc")
    return jax.shard_map(
        local,
        mesh=planes,
        in_specs=(P(sp, None), P(None, "tp"), P(None, "tp"), P(None, "tp"), P(None, "tp")),
        out_specs=(P(sp, "tp"), P("tp", sp)),
        check_vma=False,
    )
```

time: 103 us -> 70 us (0.68)
  the two profiles are of different devices: /device:TPU:304 before, /device:TPU:64 now
where the time goes in v1:
time: 70 us; the launch traced here: 69.6 us
  blocking collectives  26.6 us (38%)
  starting transfers between devices  13.9 us (20%)
  Pallas kernels  13.5 us (19%)
  waiting for transfers between devices  11.6 us (17%)
  local copies, waits for them, and re-layouts  3.26 us (5%)
  between operations  0.75 us (1%)
    all_to_all x2, blocking collectives, swap(): return lax.all_to_all(blocks, axis, split_axis=0, concat_axis=0, tiled=True)  26.6 us
    ppermute x3, waiting for transfers between devices, behind(): lax.ppermute(block, axes, [(i - distance, i) for i in range(distance, cou...  11.6 us
    ppermute x3, starting transfers between devices, behind(): lax.ppermute(block, axes, [(i - distance, i) for i in range(distance, cou...  10.4 us
    pallas_call x1, Pallas kernels, project(): pl.pallas_call(project_body, grid=(K_STEPS,), in_specs=[pl.BlockSpec((TOK...  4.86 us
    all_to_all x1, starting transfers between devices, swap(): return lax.all_to_all(blocks, axis, split_axis=0, concat_axis=0, tiled=True)  3.51 us
    unnamed x20, local copies, waits for them, and re-layouts  3.26 us
    pallas_call x1, Pallas kernels, near_middle(): pl.pallas_call(near_middle_body, in_specs=[WHOLE] * 5, out_specs=[WHOLE]...  2.46 us
    pallas_call x1, Pallas kernels, mix(): pl.pallas_call(mix_body, in_specs=[WHOLE] * 2, out_specs=WHOLE, out_shape...  2.13 us
  transfers between devices with their start and end apart: 4, of which 2 were waited for; matrix products, arithmetic and copies ran while one was open for 0% of the time, Pallas kernels for 7%

profile of v1, /device:TPU:64, one launch (start us, length us, event | category | flops | bytes accessed | tf_op | source)
XLA Modules:
  0.0 69.6 jit_solution(10208226926565489703)
XLA Ops:
  0.6 4.9 %project.1 = (bf16[16,48,128]{2,1,0:T(8,128)(2,1)S(1)}, bf16[2,256,128]{2,1,0:T(8,128)(2,1)S(1)}, bf16[2,128,128]{2,1,0:T(8,128)(2,1)S(1)}, bf16[768,128]{1,0:T(8,128)(2,1)S(1)}, bf16[512,128]{1,0:T(8,128)(2,1)S(1)}) custom-call(bf16[256,2048]{1,0:T(8,128)(2,1)} %tok.1, bf16[2048,384]{1,0:T(8,128)(2,1)} %wq.1, bf16[2048,384]{1,0:T(8,128)(2,1)} %wk.1, ...), custom_call_target="tpu_custom_call" | custom-call | tf_op jit(solution)/shard_map/project/pallas_call | solution.py:95
  5.5 0.0 copy-start.1
  5.5 0.0 copy-start
  5.5 0.0 copy-start.4
  5.5 16.9 %all_to_all.15.mine = bf16[16,48,128]{2,1,0:T(8,128)(2,1)S(1)} all-to-all(bf16[16,48,128]{2,1,0:T(8,128)(2,1)S(1)} %get-tuple-element.17), channel_id=1, replica_groups=mesh['z'=16,'yc'=16,'tp'=4] {'yc'}, dimensions={0} | all-to-all | bytes 393216 | tf_op jit(solution)/shard_map/all_to_all | solution.py:226
  22.4 0.0 copy-start.5
  22.4 4.3 %collective-permute-start.2 = (bf16[8,32,128]{2,1,0:T(8,128)(2,1)S(1)}, bf16[8,32,128]{2,1,0:T(8,128)(2,1)S(1)}, u32[]{:S(2)}, u32[]{:S(2)}) collective-permute-start(bf16[8,32,128]{2,1,0:T(8,128)(2,1)S(1)} %slice.4), channel_id=1, source_target_pairs={{0,64},{64,128},{128,192},{192,256},{256,320},{320,384},{384,448},... | collective-permute-start | bytes 196616 | tf_op jit(solution)/shard_map/ppermute | solution.py:231
  26.7 2.4 %collective-permute-start = (bf16[768,128]{1,0:T(8,128)(2,1)S(1)}, bf16[768,128]{1,0:T(8,128)(2,1)S(1)}, u32[]{:S(2)}, u32[]{:S(2)}) collective-permute-start(bf16[768,128]{1,0:T(8,128)(2,1)S(1)} %get-tuple-element.13.own), channel_id=1, source_target_pairs={{0,4},{4,8},{8,12},{12,16},{16,20},{20,24},{24,28},{28,32},{32,36}... | collective-permute-start | bytes 589832 | tf_op jit(solution)/shard_map/ppermute | solution.py:231
  29.1 5.3 %collective-permute-done.2.halo = bf16[8,32,128]{2,1,0:T(8,128)(2,1)S(1)} collective-permute-done((bf16[8,32,128]{2,1,0:T(8,128)(2,1)S(1)}, bf16[8,32,128]{2,1,0:T(8,128)(2,1)S(1)}, u32[]{:S(2)}, u32[]{:S(2)}) %collective-permute-start.2) | collective-permute-done | bytes 65568 | tf_op jit(solution)/shard_map/ppermute | solution.py:231
  34.3 0.0 copy-done.5
  34.3 0.0 copy-start.9
  34.3 0.6 copy-done.9
  35.0 2.1 %far.1 = bf16[16,24,128]{2,1,0:T(8,128)(2,1)} custom-call(bf16[16,48,128]{2,1,0:T(8,128)(2,1)} %copy-done.5, bf16[8,32,128]{2,1,0:T(8,128)(2,1)} %copy-done.9), custom_call_target="tpu_custom_call" | custom-call | tf_op jit(solution)/shard_map/far/pallas_call | solution.py:171
  37.1 3.5 %all-to-all-start.1 = ((bf16[16,24,128]{2,1,0:T(8,128)(2,1)}), bf16[16,24,128]{2,1,0:T(8,128)(2,1)S(1)}, u32[]{:S(2)}, u32[]{:S(2)}) async-start(bf16[16,24,128]{2,1,0:T(8,128)(2,1)} %far.1), calls=%async_computation.1 | async-start | bytes 196608 | tf_op jit(solution)/shard_map/all_to_all | solution.py:226
  40.6 3.7 %collective-permute-start.1 = (bf16[512,128]{1,0:T(8,128)(2,1)S(1)}, bf16[512,128]{1,0:T(8,128)(2,1)S(1)}, u32[]{:S(2)}, u32[]{:S(2)}) collective-permute-start(bf16[512,128]{1,0:T(8,128)(2,1)S(1)} %get-tuple-element.14), channel_id=1, source_target_pairs={{0,8},{4,12},{8,16},{12,20},{16,24},{20,28},{24,32},{28,36},{32,40... | collective-permute-start | bytes 393224 | tf_op jit(solution)/shard_map/ppermute | solution.py:231
  44.3 6.3 %collective-permute-done.1.two = bf16[512,128]{1,0:T(8,128)(2,1)S(1)} collective-permute-done((bf16[512,128]{1,0:T(8,128)(2,1)S(1)}, bf16[512,128]{1,0:T(8,128)(2,1)S(1)}, u32[]{:S(2)}, u32[]{:S(2)}) %collective-permute-start.1) | collective-permute-done | bytes 131104 | tf_op jit(solution)/shard_map/ppermute | solution.py:231
  50.6 0.0 copy-start.8
  50.6 0.0 collective-permute-done.one
  50.6 0.0 copy-done.1
  50.6 0.0 copy-start.7
  50.6 0.0 copy-done
  50.6 0.0 copy-done.4
  50.7 0.6 copy-done.8
  51.3 0.1 copy-done.7
  51.3 2.5 %near_middle.1 = (f32[256,128]{1,0:T(8,128)S(1)}, f32[256,128]{1,0:T(8,128)S(1)}) custom-call(bf16[2,256,128]{2,1,0:T(8,128)(2,1)} %copy-done.1, bf16[2,128,128]{2,1,0:T(8,128)(2,1)} %copy-done.4, bf16[768,128]{1,0:T(8,128)(2,1)} %copy-done, bf16[768,128]{1,0:T(8,128)(2,1)} %copy-done.7, bf16[512,128]{1,0:T(8,128)(2,1)} %copy-done.8), custom_call_target="tpu_custom_call" | custom-call | tf_op jit(solution)/shard_map/near_middle/pallas_call | solution.py:142
  53.8 0.0 copy-start.2
  53.8 0.6 copy-done.2
  54.5 0.0 copy-start.3
  54.5 0.7 copy-done.3
  55.1 0.0 all-to-all-done.1.far
  55.1 0.0 copy-start.6
  55.1 0.6 copy-done.6
  55.8 1.9 %merge.1 = (bf16[4,256,128]{2,1,0:T(8,128)(2,1)S(1)}, f32[1,256]{1,0:T(1,128)}) custom-call(f32[256,128]{1,0:T(8,128)} %copy-done.2, f32[256,128]{1,0:T(8,128)} %copy-done.3, bf16[16,24,128]{2,1,0:T(8,128)(2,1)} %copy-done.6), custom_call_target="tpu_custom_call" | custom-call | tf_op jit(solution)/shard_map/merge/pallas_call | solution.py:201
  57.7 9.7 %all_to_all.16.heads = bf16[4,256,128]{2,1,0:T(8,128)(2,1)} all-to-all(bf16[4,256,128]{2,1,0:T(8,128)(2,1)S(1)} %get-tuple-element.18), channel_id=1, replica_groups=mesh['z'=16,'yc'=16,'tp'=4] {'tp'}, dimensions={0} | all-to-all | bytes 524288 | tf_op jit(solution)/shard_map/all_to_all | solution.py:226
  67.4 2.1 %mix.1 = bf16[256,512]{1,0:T(8,128)(2,1)} custom-call(bf16[4,256,128]{2,1,0:T(8,128)(2,1)} %all_to_all.16.heads, bf16[512,512]{1,0:T(8,128)(2,1)} %weight.1), custom_call_target="tpu_custom_call" | custom-call | tf_op jit(solution)/shard_map/mix/pallas_call | solution.py:216
  (1 shorter events, 0.0 us)
Async XLA Ops:
  5.5 45.1 %copy-start.1 = (bf16[2,256,128]{2,1,0:T(8,128)(2,1)}, bf16[2,256,128]{2,1,0:T(8,128)(2,1)S(1)}, u32[]{:S(2)}) copy-start(bf16[2,256,128]{2,1,0:T(8,128)(2,1)S(1)} %get-tuple-element.11.queries) | copy-start | bytes 393220
  5.5 45.1 %copy-start = (bf16[768,128]{1,0:T(8,128)(2,1)}, bf16[768,128]{1,0:T(8,128)(2,1)S(1)}, u32[]{:S(2)}) copy-start(bf16[768,128]{1,0:T(8,128)(2,1)S(1)} %get-tuple-element.13.own) | copy-start | bytes 589828
  5.5 45.1 %copy-start.4 = (bf16[2,128,128]{2,1,0:T(8,128)(2,1)}, bf16[2,128,128]{2,1,0:T(8,128)(2,1)S(1)}, u32[]{:S(2)}) copy-start(bf16[2,128,128]{2,1,0:T(8,128)(2,1)S(1)} %get-tuple-element.12.near) | copy-start | bytes 196612
  22.4 11.9 %copy-start.5 = (bf16[16,48,128]{2,1,0:T(8,128)(2,1)}, bf16[16,48,128]{2,1,0:T(8,128)(2,1)S(1)}, u32[]{:S(2)}) copy-start(bf16[16,48,128]{2,1,0:T(8,128)(2,1)S(1)} %all_to_all.15.mine) | copy-start | bytes 589828
  22.4 11.9 %collective-permute-start.2 = (bf16[8,32,128]{2,1,0:T(8,128)(2,1)S(1)}, bf16[8,32,128]{2,1,0:T(8,128)(2,1)S(1)}, u32[]{:S(2)}, u32[]{:S(2)}) collective-permute-start(bf16[8,32,128]{2,1,0:T(8,128)(2,1)S(1)} %slice.4), channel_id=1, source_target_pairs={{0,64},{64,128},{128,192},{192,256},{256,320},{320,384},{384,448},... | collective-permute-start | bytes 196616 | tf_op jit(solution)/shard_map/ppermute | solution.py:231
  26.7 23.9 %collective-permute-start = (bf16[768,128]{1,0:T(8,128)(2,1)S(1)}, bf16[768,128]{1,0:T(8,128)(2,1)S(1)}, u32[]{:S(2)}, u32[]{:S(2)}) collective-permute-start(bf16[768,128]{1,0:T(8,128)(2,1)S(1)} %get-tuple-element.13.own), channel_id=1, source_target_pairs={{0,4},{4,8},{8,12},{12,16},{16,20},{20,24},{24,28},{28,32},{32,36}... | collective-permute-start | bytes 589832 | tf_op jit(solution)/shard_map/ppermute | solution.py:231
  34.3 0.6 copy-start.9
  37.1 18.0 %all-to-all-start.1 = ((bf16[16,24,128]{2,1,0:T(8,128)(2,1)}), bf16[16,24,128]{2,1,0:T(8,128)(2,1)S(1)}, u32[]{:S(2)}, u32[]{:S(2)}) async-start(bf16[16,24,128]{2,1,0:T(8,128)(2,1)} %far.1), calls=%async_computation.1 | async-start | bytes 196608 | tf_op jit(solution)/shard_map/all_to_all | solution.py:226
  40.6 10.0 %collective-permute-start.1 = (bf16[512,128]{1,0:T(8,128)(2,1)S(1)}, bf16[512,128]{1,0:T(8,128)(2,1)S(1)}, u32[]{:S(2)}, u32[]{:S(2)}) collective-permute-start(bf16[512,128]{1,0:T(8,128)(2,1)S(1)} %get-tuple-element.14), channel_id=1, source_target_pairs={{0,8},{4,12},{8,16},{12,20},{16,24},{20,28},{24,32},{28,36},{32,40... | collective-permute-start | bytes 393224 | tf_op jit(solution)/shard_map/ppermute | solution.py:231
  50.6 0.6 copy-start.8
  50.6 0.7 %copy-start.7 = (bf16[768,128]{1,0:T(8,128)(2,1)}, bf16[768,128]{1,0:T(8,128)(2,1)S(1)}, u32[]{:S(2)}) copy-start(bf16[768,128]{1,0:T(8,128)(2,1)S(1)} %collective-permute-done.one) | copy-start | bytes 589828
  53.8 0.7 copy-start.2
  54.5 0.7 copy-start.3
  55.1 0.6 copy-start.6

commit v2 on v1

--- a/solution.py
+++ b/solution.py
@@ -13,11 +13,14 @@
 BAND = 128
 MIDDLE_DILATION = 4
 SCALE = HEAD_DIM**-0.5
-K_STEPS = 4
 F32 = jnp.float32
 BF16 = jnp.bfloat16
 VMEM = pltpu.VMEM
 WHOLE = pl.BlockSpec(memory_space=pltpu.VMEM)
+
+
+def held(*arrays):
+    return [pltpu.with_memory_space_constraint(a, pltpu.VMEM) for a in arrays]
 
 
 def iota(shape, dim):
@@ -56,46 +59,61 @@
     return soft(scores, valid, values)
 
 
-def project_body(tok, wq, wk, wv, far, queries, near, sent_one, sent_two, acc):
-    step = pl.program_id(0)
-
-    @pl.when(step == 0)
-    def _():
-        acc[...] = jnp.zeros_like(acc)
-
-    x = tok[...]
-    for j, w in enumerate((wq, wk, wv)):
-        acc[j] += jnp.dot(x, w[...], preferred_element_type=F32)
-
-    @pl.when(step == pl.num_programs(0) - 1)
-    def _():
-        q, k, v = acc[0].astype(BF16), acc[1].astype(BF16), acc[2].astype(BF16)
-        d = HEAD_DIM
-        order = residue_order()
-        for j, part in enumerate((q, k, v)):
-            sorted_rows = jnp.dot(order, part[:, 2 * d :], preferred_element_type=F32).astype(BF16)
-            far[:, j * RUN : (j + 1) * RUN] = sorted_rows.reshape(PLANE, RUN, d)
-        queries[0] = q[:, :d]
-        queries[1] = q[:, d : 2 * d]
-        near[0] = k[:BAND, :d]
-        near[1] = v[:BAND, :d]
-        sent_one[:BAND] = k[BAND:, :d]
-        sent_one[BAND : 2 * BAND] = v[BAND:, :d]
-        for j, part in enumerate((k, v)):
-            rows = part[:, d : 2 * d]
-            sent_one[2 * BAND + j * TOK : 2 * BAND + (j + 1) * TOK] = rows
-            sent_two[j * TOK : (j + 1) * TOK] = rows
+def project_body(tok_hbm, wq_hbm, wk_hbm, wv_hbm, far, queries, near, sent_one, sent_two, tok, wq, wk, wv, sems):
+    pairs = ((tok_hbm, tok), (wk_hbm, wk), (wv_hbm, wv), (wq_hbm, wq))
+    copies = []
+    for j, (source, target) in enumerate(pairs):
+        half = source.shape[0] // 2
+        parts = [
+            pltpu.make_async_copy(source.at[pl.ds(i * half, half)], target.at[pl.ds(i * half, half)], sems.at[j, i])
+            for i in range(2)
+        ]
+        for part in parts:
+            part.start()
+        copies.append(parts)
+
+    def arrive(j):
+        for part in copies[j]:
+            part.wait()
+
+    def times(weight):
+        return jnp.dot(tok[...], weight[...], preferred_element_type=F32).astype(BF16)
+
+    d = HEAD_DIM
+    order = residue_order()
+
+    def put_far(j, rows):
+        rows = jnp.dot(order, rows[:, 2 * d :], preferred_element_type=F32).astype(BF16)
+        far[:, j * RUN : (j + 1) * RUN] = rows.reshape(PLANE, RUN, d)
+
+    def put_sent(j, rows):
+        near[j] = rows[:BAND, :d]
+        sent_one[j * BAND : (j + 1) * BAND] = rows[BAND:, :d]
+        sent_one[2 * BAND + j * TOK : 2 * BAND + (j + 1) * TOK] = rows[:, d : 2 * d]
+        sent_two[j * TOK : (j + 1) * TOK] = rows[:, d : 2 * d]
+
+    arrive(0)
+    arrive(1)
+    rows = times(wk)
+    put_far(1, rows)
+    put_sent(0, rows)
+    arrive(2)
+    rows = times(wv)
+    put_far(2, rows)
+    put_sent(1, rows)
+    arrive(3)
+    rows = times(wq)
+    put_far(0, rows)
+    queries[0] = rows[:, :d]
+    queries[1] = rows[:, d : 2 * d]
 
 
 def project(tokens, wq, wk, wv):
-    width, cols = wq.shape
-    chunk = width // K_STEPS
     d = HEAD_DIM
-    weight = pl.BlockSpec((chunk, cols), lambda i: (i, 0))
+    in_hbm = pl.BlockSpec(memory_space=pl.ANY)
     return pl.pallas_call(
         project_body,
-        grid=(K_STEPS,),
-        in_specs=[pl.BlockSpec((TOK, chunk), lambda i: (0, i)), weight, weight, weight],
+        in_specs=[in_hbm] * 4,
         out_specs=[WHOLE] * 5,
         out_shape=[
             VMEM((PLANE, 3 * RUN, d), BF16),
@@ -104,9 +122,9 @@
             VMEM((2 * BAND + 2 * TOK, d), BF16),
             VMEM((2 * TOK, d), BF16),
         ],
-        scratch_shapes=[pltpu.VMEM((3, TOK, cols), F32)],
+        scratch_shapes=[pltpu.VMEM(a.shape, a.dtype) for a in (tokens, wq, wk, wv)] + [pltpu.SemaphoreType.DMA((4, 2))],
         name="project",
-    )(tokens, wq, wk, wv)
+    )(*[pltpu.with_memory_space_constraint(a, pltpu.HBM) for a in (tokens, wq, wk, wv)])
 
 
 def near_middle_body(queries, near, own, one, two, attended, log):
@@ -145,7 +163,7 @@
         out_specs=[WHOLE] * 2,
         out_shape=[VMEM(shape, F32), VMEM(shape, F32)],
         name="near_middle",
-    )(queries, near, own, one, two)
+    )(*held(queries, near, own, one, two))
 
 
 def far_body(mine, halo, out):
@@ -174,7 +192,7 @@
         out_specs=WHOLE,
         out_shape=VMEM((PLANE, RUN + 8, HEAD_DIM), BF16),
         name="far",
-    )(mine, halo)
+    )(*held(mine, halo))
 
 
 def merge_body(attended, log, far, merged, total_log):
@@ -202,9 +220,9 @@
         merge_body,
         in_specs=[WHOLE] * 3,
         out_specs=[WHOLE] * 2,
-        out_shape=[VMEM((copies, TOK, HEAD_DIM), BF16), jax.ShapeDtypeStruct((1, TOK), F32)],
+        out_shape=[VMEM((copies, TOK, HEAD_DIM), BF16), VMEM((1, TOK), F32)],
         name="merge",
-    )(attended, log, far)
+    )(*held(attended, log, far))
 
 
 def mix_body(heads, weight, out):
@@ -219,7 +237,7 @@
         out_specs=WHOLE,
         out_shape=jax.ShapeDtypeStruct((TOK, weight.shape[1]), BF16),
         name="mix",
-    )(heads, weight)
+    )(*held(heads, weight))
 
 
 def swap(blocks, axis):

time: 70 us -> 62.5 us (0.89)
  blocking collectives: 26.6 us -> 17 us
  waiting for transfers between devices: 11.6 us -> 17.6 us
  Pallas kernels: 13.5 us -> 8.96 us
  starting transfers between devices: 13.9 us -> 17.3 us
  local copies, waits for them, and re-layouts: 3.26 us -> 0.58 us
    all_to_all x2 -> x1, blocking collectives: 26.6 us -> 17 us  [swap(): return lax.all_to_all(blocks, axis, split_axis=0, concat_axis=0, tiled=True)]
    all_to_all x1 -> x2, waiting for transfers between devices: 0.01 us -> 6.08 us  [swap(): return lax.all_to_all(blocks, axis, split_axis=0, concat_axis=0, tiled=True)]
    all_to_all x1 -> x2, starting transfers between devices: 3.51 us -> 6.91 us  [swap(): return lax.all_to_all(blocks, axis, split_axis=0, concat_axis=0, tiled=True)]
    unnamed x20 -> x3, local copies, waits for them, and re-layouts: 3.26 us -> 0.57 us
    pallas_call x1, Pallas kernels: 2.46 us -> 1.27 us  [near_middle(): pl.pallas_call(near_middle_body, in_specs=[WHOLE] * 5, out_specs=[WHOLE]...]
    pallas_call x1, Pallas kernels: 2.13 us -> 1.01 us  [mix(): pl.pallas_call(mix_body, in_specs=[WHOLE] * 2, out_specs=WHOLE, out_shape...]
    pallas_call x1, Pallas kernels: 2.13 us -> 1.2 us  [far_attention(): pl.pallas_call(far_body, in_specs=[WHOLE] * 2, out_specs=WHOLE, out_shape...]
    pallas_call x1, Pallas kernels: 1.94 us -> 1.02 us  [merge(): pl.pallas_call(merge_body, in_specs=[WHOLE] * 3, out_specs=[WHOLE] * 2, o...]
  transfers between devices with their start and end apart: 4 -> 5, of which waited for: 2 -> 3; matrix products, arithmetic and copies ran while one was open for 0% -> 1% of each run, Pallas kernels for 7% -> 4%
where the time goes in v2:
time: 62.5 us; the launch traced here: 62.1 us
  waiting for transfers between devices  17.6 us (28%)
  starting transfers between devices  17.3 us (28%)
  blocking collectives  17 us (27%)
  Pallas kernels  8.96 us (14%)
  between operations  0.7 us (1%)
    all_to_all x1, blocking collectives, swap(): return lax.all_to_all(blocks, axis, split_axis=0, concat_axis=0, tiled=True)  17 us
    ppermute x3, waiting for transfers between devices, behind(): lax.ppermute(block, axes, [(i - distance, i) for i in range(distance, cou...  11.6 us
    ppermute x3, starting transfers between devices, behind(): lax.ppermute(block, axes, [(i - distance, i) for i in range(distance, cou...  10.3 us
    all_to_all x2, starting transfers between devices, swap(): return lax.all_to_all(blocks, axis, split_axis=0, concat_axis=0, tiled=True)  6.91 us
    all_to_all x2, waiting for transfers between devices, swap(): return lax.all_to_all(blocks, axis, split_axis=0, concat_axis=0, tiled=True)  6.08 us
    pallas_call x1, Pallas kernels, project(): pl.pallas_call(project_body, in_specs=[in_hbm] * 4, out_specs=[WHOLE] * 5...  4.46 us
    pallas_call x1, Pallas kernels, near_middle(): pl.pallas_call(near_middle_body, in_specs=[WHOLE] * 5, out_specs=[WHOLE]...  1.27 us
  transfers between devices with their start and end apart: 5, of which 3 were waited for; matrix products, arithmetic and copies ran while one was open for 1% of the time, Pallas kernels for 4%

profile of v2, /device:TPU:64, one launch (start us, length us, event | category | flops | bytes accessed | tf_op | source)
XLA Modules:
  0.0 62.1 jit_solution(315868452630546851)
XLA Ops:
  0.6 4.5 %project.1 = (bf16[16,48,128]{2,1,0:T(8,128)(2,1)S(1)}, bf16[2,256,128]{2,1,0:T(8,128)(2,1)S(1)}, bf16[2,128,128]{2,1,0:T(8,128)(2,1)S(1)}, bf16[768,128]{1,0:T(8,128)(2,1)S(1)}, bf16[512,128]{1,0:T(8,128)(2,1)S(1)}) custom-call(bf16[256,2048]{1,0:T(8,128)(2,1)} %tok_hbm.1, bf16[2048,384]{1,0:T(8,128)(2,1)} %wq_hbm.1, bf16[2048,384]{1,0:T(8,128)(2,1)} %wk_hbm.1, ...), custom_call_target="tpu_custom_call" | custom-call | tf_op jit(solution)/shard_map/project/pallas_call | solution.py:114
  5.1 0.0 copy-start
  5.1 17.0 %all_to_all.15.mine = bf16[16,48,128]{2,1,0:T(8,128)(2,1)S(1)} all-to-all(bf16[16,48,128]{2,1,0:T(8,128)(2,1)S(1)} %get-tuple-element.17), channel_id=1, replica_groups=mesh['z'=16,'yc'=16,'tp'=4] {'yc'}, dimensions={0} | all-to-all | bytes 393216 | tf_op jit(solution)/shard_map/all_to_all | solution.py:244
  22.1 4.3 %collective-permute-start.2 = (bf16[8,32,128]{2,1,0:T(8,128)(2,1)S(1)}, bf16[8,32,128]{2,1,0:T(8,128)(2,1)S(1)}, u32[]{:S(2)}, u32[]{:S(2)}) collective-permute-start(bf16[8,32,128]{2,1,0:T(8,128)(2,1)S(1)} %slice.4), channel_id=1, source_target_pairs={{0,64},{64,128},{128,192},{192,256},{256,320},{320,384},{384,448},... | collective-permute-start | bytes 196616 | tf_op jit(solution)/shard_map/ppermute | solution.py:249
  26.4 2.4 %collective-permute-start = (bf16[768,128]{1,0:T(8,128)(2,1)S(1)}, bf16[768,128]{1,0:T(8,128)(2,1)S(1)}, u32[]{:S(2)}, u32[]{:S(2)}) collective-permute-start(bf16[768,128]{1,0:T(8,128)(2,1)S(1)} %get-tuple-element.13.own), channel_id=1, source_target_pairs={{0,4},{4,8},{8,12},{12,16},{16,20},{20,24},{24,28},{28,32},{32,36}... | collective-permute-start | bytes 589832 | tf_op jit(solution)/shard_map/ppermute | solution.py:249
  28.8 5.3 %collective-permute-done.2.halo = bf16[8,32,128]{2,1,0:T(8,128)(2,1)S(1)} collective-permute-done((bf16[8,32,128]{2,1,0:T(8,128)(2,1)S(1)}, bf16[8,32,128]{2,1,0:T(8,128)(2,1)S(1)}, u32[]{:S(2)}, u32[]{:S(2)}) %collective-permute-start.2) | collective-permute-done | bytes 65568 | tf_op jit(solution)/shard_map/ppermute | solution.py:249
  34.0 1.2 %far.1 = bf16[16,24,128]{2,1,0:T(8,128)(2,1)} custom-call(bf16[16,48,128]{2,1,0:T(8,128)(2,1)S(1)} %all_to_all.15.mine, bf16[8,32,128]{2,1,0:T(8,128)(2,1)S(1)} %collective-permute-done.2.halo), custom_call_target="tpu_custom_call" | custom-call | tf_op jit(solution)/shard_map/far/pallas_call | solution.py:189
  35.2 3.5 %all-to-all-start.1 = ((bf16[16,24,128]{2,1,0:T(8,128)(2,1)}), bf16[16,24,128]{2,1,0:T(8,128)(2,1)S(1)}, u32[]{:S(2)}, u32[]{:S(2)}) async-start(bf16[16,24,128]{2,1,0:T(8,128)(2,1)} %far.1), calls=%async_computation.1 | async-start | bytes 196608 | tf_op jit(solution)/shard_map/all_to_all | solution.py:244
  38.8 3.7 %collective-permute-start.1 = (bf16[512,128]{1,0:T(8,128)(2,1)S(1)}, bf16[512,128]{1,0:T(8,128)(2,1)S(1)}, u32[]{:S(2)}, u32[]{:S(2)}) collective-permute-start(bf16[512,128]{1,0:T(8,128)(2,1)S(1)} %get-tuple-element.14), channel_id=1, source_target_pairs={{0,8},{4,12},{8,16},{12,20},{16,24},{20,28},{24,32},{28,36},{32,40... | collective-permute-start | bytes 393224 | tf_op jit(solution)/shard_map/ppermute | solution.py:249
  42.5 6.3 %collective-permute-done.1.two = bf16[512,128]{1,0:T(8,128)(2,1)S(1)} collective-permute-done((bf16[512,128]{1,0:T(8,128)(2,1)S(1)}, bf16[512,128]{1,0:T(8,128)(2,1)S(1)}, u32[]{:S(2)}, u32[]{:S(2)}) %collective-permute-start.1) | collective-permute-done | bytes 131104 | tf_op jit(solution)/shard_map/ppermute | solution.py:249
  48.8 0.0 collective-permute-done.one
  48.8 1.3 %near_middle.1 = (f32[256,128]{1,0:T(8,128)S(1)}, f32[256,128]{1,0:T(8,128)S(1)}) custom-call(bf16[2,256,128]{2,1,0:T(8,128)(2,1)S(1)} %get-tuple-element.11.queries, bf16[2,128,128]{2,1,0:T(8,128)(2,1)S(1)} %get-tuple-element.12.near, bf16[768,128]{1,0:T(8,128)(2,1)S(1)} %get-tuple-element.13.own, bf16[768,128]{1,0:T(8,128)(2,1)S(1)} %collective-permute-done.one, ...), custom_call_target="tpu_custom_call" | custom-call | tf_op jit(solution)/shard_map/near_middle/pallas_call | solution.py:160
  50.0 0.0 all-to-all-done.1.far
  50.1 1.0 %merge.1 = (bf16[4,256,128]{2,1,0:T(8,128)(2,1)}, f32[1,256]{1,0:T(1,128)S(1)}) custom-call(f32[256,128]{1,0:T(8,128)S(1)} %get-tuple-element.15.attended, f32[256,128]{1,0:T(8,128)S(1)} %get-tuple-element.16.log, bf16[16,24,128]{2,1,0:T(8,128)(2,1)S(1)} %all-to-all-done.1.far), custom_call_target="tpu_custom_call" | custom-call | tf_op jit(solution)/shard_map/merge/pallas_call | solution.py:219
  51.1 3.4 %all-to-all-start.2 = ((bf16[4,256,128]{2,1,0:T(8,128)(2,1)}), bf16[4,256,128]{2,1,0:T(8,128)(2,1)S(1)}, u32[]{:S(2)}, u32[]{:S(2)}) async-start(bf16[4,256,128]{2,1,0:T(8,128)(2,1)} %get-tuple-element.18), calls=%async_computation.2 | async-start | bytes 524288 | tf_op jit(solution)/shard_map/all_to_all | solution.py:244
  54.5 0.6 copy.7
  55.1 6.1 %all-to-all-done.2.heads = bf16[4,256,128]{2,1,0:T(8,128)(2,1)S(1)} async-done(((bf16[4,256,128]{2,1,0:T(8,128)(2,1)}), bf16[4,256,128]{2,1,0:T(8,128)(2,1)S(1)}, u32[]{:S(2)}, u32[]{:S(2)}) %all-to-all-start.2) | async-done | bytes 262176 | tf_op jit(solution)/shard_map/all_to_all | solution.py:244
  61.1 0.0 copy-done
  61.1 1.0 %mix.1 = bf16[256,512]{1,0:T(8,128)(2,1)} custom-call(bf16[4,256,128]{2,1,0:T(8,128)(2,1)S(1)} %all-to-all-done.2.heads, bf16[512,512]{1,0:T(8,128)(2,1)S(1)} %copy-done), custom_call_target="tpu_custom_call" | custom-call | tf_op jit(solution)/shard_map/mix/pallas_call | solution.py:234
  (1 shorter events, 0.0 us)
Async XLA Ops:
  5.1 56.0 %copy-start = (bf16[512,512]{1,0:T(8,128)(2,1)S(1)}, bf16[512,512]{1,0:T(8,128)(2,1)}, u32[]{:S(2)}) copy-start(bf16[512,512]{1,0:T(8,128)(2,1)} %weight.1) | copy-start | bytes 1572868
  22.1 11.9 %collective-permute-start.2 = (bf16[8,32,128]{2,1,0:T(8,128)(2,1)S(1)}, bf16[8,32,128]{2,1,0:T(8,128)(2,1)S(1)}, u32[]{:S(2)}, u32[]{:S(2)}) collective-permute-start(bf16[8,32,128]{2,1,0:T(8,128)(2,1)S(1)} %slice.4), channel_id=1, source_target_pairs={{0,64},{64,128},{128,192},{192,256},{256,320},{320,384},{384,448},... | collective-permute-start | bytes 196616 | tf_op jit(solution)/shard_map/ppermute | solution.py:249
  26.4 22.4 %collective-permute-start = (bf16[768,128]{1,0:T(8,128)(2,1)S(1)}, bf16[768,128]{1,0:T(8,128)(2,1)S(1)}, u32[]{:S(2)}, u32[]{:S(2)}) collective-permute-start(bf16[768,128]{1,0:T(8,128)(2,1)S(1)} %get-tuple-element.13.own), channel_id=1, source_target_pairs={{0,4},{4,8},{8,12},{12,16},{16,20},{20,24},{24,28},{28,32},{32,36}... | collective-permute-start | bytes 589832 | tf_op jit(solution)/shard_map/ppermute | solution.py:249
  35.2 14.8 %all-to-all-start.1 = ((bf16[16,24,128]{2,1,0:T(8,128)(2,1)}), bf16[16,24,128]{2,1,0:T(8,128)(2,1)S(1)}, u32[]{:S(2)}, u32[]{:S(2)}) async-start(bf16[16,24,128]{2,1,0:T(8,128)(2,1)} %far.1), calls=%async_computation.1 | async-start | bytes 196608 | tf_op jit(solution)/shard_map/all_to_all | solution.py:244
  38.8 10.0 %collective-permute-start.1 = (bf16[512,128]{1,0:T(8,128)(2,1)S(1)}, bf16[512,128]{1,0:T(8,128)(2,1)S(1)}, u32[]{:S(2)}, u32[]{:S(2)}) collective-permute-start(bf16[512,128]{1,0:T(8,128)(2,1)S(1)} %get-tuple-element.14), channel_id=1, source_target_pairs={{0,8},{4,12},{8,16},{12,20},{16,24},{20,28},{24,32},{28,36},{32,40... | collective-permute-start | bytes 393224 | tf_op jit(solution)/shard_map/ppermute | solution.py:249
  51.1 10.1 %all-to-all-start.2 = ((bf16[4,256,128]{2,1,0:T(8,128)(2,1)}), bf16[4,256,128]{2,1,0:T(8,128)(2,1)S(1)}, u32[]{:S(2)}, u32[]{:S(2)}) async-start(bf16[4,256,128]{2,1,0:T(8,128)(2,1)} %get-tuple-element.18), calls=%async_computation.2 | async-start | bytes 524288 | tf_op jit(solution)/shard_map/all_to_all | solution.py:244

commit v3 on v2

v3 whole, which is shorter than its diff:
```python
import jax
import jax.numpy as jnp
from jax import lax
from jax.experimental import pallas as pl
from jax.experimental.pallas import tpu as pltpu
from jax.sharding import Mesh
from jax.sharding import PartitionSpec as P

HEAD_DIM = 128
TOK = 256
PLANE = 16
BAND = 128
MIDDLE_DILATION = 4
FAR_DILATION = 16
REACH = 8
SCALE = HEAD_DIM**-0.5
F32 = jnp.float32
BF16 = jnp.bfloat16
VMEM = pltpu.VMEM
WHOLE = pl.BlockSpec(memory_space=pltpu.VMEM)


def held(*arrays):
    return [pltpu.with_memory_space_constraint(a, pltpu.VMEM) for a in arrays]


def iota(shape, dim):
    return lax.broadcasted_iota(jnp.int32, shape, dim)


def head_slope():
    head = lax.axis_index("tp")
    return jnp.where(head == 0, 2.0, jnp.where(head == 1, 0.5, jnp.where(head == 2, 0.125, 0.03125)))


def times_transposed(a, b):
    return lax.dot_general(a, b, (((1,), (1,)), ((), ())), preferred_element_type=F32)


def soft(scores, valid, values):
    scores = jnp.where(valid, scores, -jnp.inf)
    highest = jnp.max(scores, axis=1, keepdims=True)
    weights = jnp.exp(scores - highest)
    total = jnp.sum(weights, axis=1, keepdims=True)
    probs = (weights * (1.0 / total)).astype(BF16)
    return jnp.dot(probs, values, preferred_element_type=F32), highest + jnp.log(total)


def banded(queries, keys, values, slope, has_prior):
    shape = (TOK, TOK + BAND)
    spacing = iota(shape, 0) + BAND - iota(shape, 1)
    first = jnp.where(has_prior, 0, BAND)
    valid = (spacing >= 0) & (spacing <= BAND) & (iota(shape, 1) >= first)
    scores = times_transposed(queries, keys) * SCALE - slope * spacing.astype(F32)
    return soft(scores, valid, values)


def project_body(tok_hbm, wq_hbm, wk_hbm, wv_hbm, queries, near, far, pack, tok, wq, wk, wv, sems):
    pairs = ((tok_hbm, tok), (wk_hbm, wk), (wv_hbm, wv), (wq_hbm, wq))
    copies = []
    for j, (source, target) in enumerate(pairs):
        half = source.shape[0] // 2
        parts = [
            pltpu.make_async_copy(source.at[pl.ds(i * half, half)], target.at[pl.ds(i * half, half)], sems.at[j, i])
            for i in range(2)
        ]
        for part in parts:
            part.start()
        copies.append(parts)

    def arrive(j):
        for part in copies[j]:
            part.wait()

    d = HEAD_DIM
    arrive(0)
    for j, weight in enumerate((wk, wv)):
        arrive(j + 1)
        rows = jnp.dot(tok[...], weight[...], preferred_element_type=F32).astype(BF16)
        far[j * TOK : (j + 1) * TOK] = rows[:, 2 * d :]
        pack[j * TOK : (j + 1) * TOK] = rows[:, 2 * d :]
        pack[(2 + j) * TOK : (3 + j) * TOK] = rows[:, d : 2 * d]
        near[j] = rows[:BAND, :d]
        pack[4 * TOK + j * BAND : 4 * TOK + (j + 1) * BAND] = rows[BAND:, :d]
    arrive(3)
    rows = jnp.dot(tok[...], wq[...], preferred_element_type=F32).astype(BF16)
    for j in range(3):
        queries[j] = rows[:, j * d : (j + 1) * d]


def project(tokens, wq, wk, wv):
    d = HEAD_DIM
    return pl.pallas_call(
        project_body,
        in_specs=[pl.BlockSpec(memory_space=pl.ANY)] * 4,
        out_specs=[WHOLE] * 4,
        out_shape=[
            VMEM((3, TOK, d), BF16),
            VMEM((2, BAND, d), BF16),
            VMEM((2 * TOK, d), BF16),
            VMEM((4 * TOK + 2 * BAND, d), BF16),
        ],
        scratch_shapes=[pltpu.VMEM(a.shape, a.dtype) for a in (tokens, wq, wk, wv)] + [pltpu.SemaphoreType.DMA((4, 2))],
        name="project",
    )(*[pltpu.with_memory_space_constraint(a, pltpu.HBM) for a in (tokens, wq, wk, wv)])


class Far:
    def __init__(self, queries, slope, place):
        self.queries, self.slope, self.place = queries, slope / (FAR_DILATION * BAND), place
        self.apart = iota((TOK, TOK), 0) - iota((TOK, TOK), 1)
        self.bias = jnp.where(self.apart % FAR_DILATION == 0, self.slope * self.apart.astype(F32), jnp.inf)

    def scores(self, places, keys):
        ahead = jnp.where(self.place >= places, self.slope * (TOK * places), jnp.inf)
        part = times_transposed(self.queries, keys) * SCALE - self.bias - ahead
        if places == 0:
            part = jnp.where(self.apart >= 0, part, -jnp.inf)
        if places == REACH:
            part = jnp.where(self.apart <= 0, part, -jnp.inf)
        return part

    def gather(self, blocks, highest=None):
        scores = [self.scores(places, ref[at : at + TOK]) for places, ref, at in blocks]
        top = scores[0]
        for part in scores[1:]:
            top = jnp.maximum(top, part)
        top = jnp.max(top, axis=1, keepdims=True)
        highest = top if highest is None else jnp.maximum(highest, top)
        total, rows = None, None
        for part, (_, ref, at) in zip(scores, blocks):
            weight = jnp.exp(part - highest)
            piece = jnp.dot(weight.astype(BF16), ref[at + TOK : at + 2 * TOK], preferred_element_type=F32)
            total = weight if total is None else total + weight
            rows = piece if rows is None else rows + piece
        return highest, jnp.sum(total, axis=1, keepdims=True), rows


def place_here():
    return lax.axis_index("z") * PLANE + lax.axis_index("yc")


def first_body(queries, near, own, one, two, four, attended, far_rows, stats):
    slope = head_slope()
    place = place_here()
    b, at = BAND, 4 * TOK
    keys = jnp.concatenate((one[at : at + b], near[0], own[at : at + b]), axis=0)
    values = jnp.concatenate((one[at + b : at + 2 * b], near[1], own[at + b : at + 2 * b]), axis=0)
    first, first_log = banded(queries[0], keys, values, slope / b, place > 0)

    k_at, v_at = slice(2 * TOK, 3 * TOK), slice(3 * TOK, 4 * TOK)
    keys = jnp.concatenate((two[k_at], one[k_at], own[k_at]), axis=0)
    values = jnp.concatenate((two[v_at], one[v_at], own[v_at]), axis=0)
    shape = (TOK, 3 * TOK)
    window = MIDDLE_DILATION * BAND
    spacing = iota(shape, 0) + window - iota(shape, 1)
    begin = jnp.maximum(window - place * TOK, 0)
    valid = (spacing >= 0) & (spacing <= window) & (spacing % MIDDLE_DILATION == 0)
    valid = valid & (iota(shape, 1) >= begin)
    scores = times_transposed(queries[1], keys) * SCALE - (slope / window) * spacing.astype(F32)
    second, second_log = soft(scores, valid, values)

    highest = jnp.maximum(first_log, second_log)
    first_share, second_share = jnp.exp(first_log - highest), jnp.exp(second_log - highest)
    total = first_share + second_share
    inverse = 1.0 / total
    attended[...] = (first_share * inverse) * first + (second_share * inverse) * second
    log = highest + jnp.log(total)

    blocks = ((0, own, 0), (1, one, 0), (2, two, 0), (3, one, 4 * TOK + 2 * BAND), (4, four, 0))
    highest, total, rows = Far(queries[2], slope, place).gather(blocks)
    far_rows[...] = rows
    lanes = iota(stats.shape, 1)
    stats[...] = jnp.where(lanes == 0, log, jnp.where(lanes == 1, highest, total))


def first(*arrays):
    shape = (TOK, HEAD_DIM)
    return pl.pallas_call(
        first_body,
        in_specs=[WHOLE] * len(arrays),
        out_specs=[WHOLE] * 3,
        out_shape=[VMEM(shape, F32)] * 3,
        name="first",
    )(*held(*arrays))


def finish_body(queries, odd, six, eight, attended, far_rows, stats, mix_hbm, merged, total_log, mix_weight, sem):
    d = HEAD_DIM
    fetch = pltpu.make_async_copy(mix_hbm, mix_weight, sem)
    fetch.start()
    blocks = ((5, odd, 0), (6, six, 0), (7, odd, 2 * TOK), (8, eight, 0))
    other_log, before, sum_before = stats[:, 0:1], stats[:, 1:2], stats[:, 2:3]
    highest, total, rows = Far(queries[2], head_slope(), place_here()).gather(blocks, before)
    kept = jnp.exp(before - highest)
    total = total + kept * sum_before
    rows = (rows + kept * far_rows[...]) * (1.0 / total)
    far_log = highest + jnp.log(total)

    highest = jnp.maximum(other_log, far_log)
    total = highest + jnp.log(jnp.exp(other_log - highest) + jnp.exp(far_log - highest))
    both = jnp.exp(other_log - total) * attended[...] + jnp.exp(far_log - total) * rows
    both = both.astype(BF16)
    for j in range(merged.shape[0]):
        merged[j] = both
    tokens, lanes = iota((TOK, d), 0), iota((TOK, d), 1)
    for j in range(TOK // d):
        part = jnp.where(lanes == tokens - j * d, total, 0.0)
        total_log[:, j * d : (j + 1) * d] = jnp.sum(part, axis=0, keepdims=True)
    fetch.wait()


def finish(copies, weight, *arrays):
    return pl.pallas_call(
        finish_body,
        in_specs=[WHOLE] * len(arrays) + [pl.BlockSpec(memory_space=pl.ANY)],
        out_specs=[WHOLE] * 3,
        out_shape=[VMEM((copies, TOK, HEAD_DIM), BF16), VMEM((1, TOK), F32), VMEM(weight.shape, BF16)],
        scratch_shapes=[pltpu.SemaphoreType.DMA],
        name="finish",
    )(*held(*arrays), pltpu.with_memory_space_constraint(weight, pltpu.HBM))


def mix_body(heads, weight, log, out, total_log):
    rows = jnp.concatenate([heads[j] for j in range(heads.shape[0])], axis=1)
    out[...] = jnp.dot(rows, weight[...], preferred_element_type=F32).astype(BF16)
    total_log[...] = log[...]


def mix(heads, weight, log):
    return pl.pallas_call(
        mix_body,
        in_specs=[WHOLE] * 3,
        out_specs=[WHOLE] * 2,
        out_shape=[jax.ShapeDtypeStruct((TOK, weight.shape[1]), BF16), jax.ShapeDtypeStruct(log.shape, F32)],
        name="mix",
    )(*held(heads, weight, log))


def swap(blocks, axis):
    return lax.all_to_all(blocks, axis, split_axis=0, concat_axis=0, tiled=True)


SP = ("z", "yc")


def behind(block, distance):
    count = lax.axis_size(SP)
    return lax.ppermute(block, SP, [(i - distance, i) for i in range(distance, count)])


def other_core(block):
    return lax.ppermute(block, SP, [(i, i ^ 1) for i in range(lax.axis_size(SP))])


def round_the_back(block):
    count = lax.axis_size(SP)

    def chip(z, y, core):
        return z * PLANE + (y % 8) * 2 + core

    places = [(z, y, core) for z in range(count // PLANE) for y in range(8) for core in range(2)]
    block = lax.ppermute(block, SP, [(chip(z, y, core), chip(z, y - 2, core)) for z, y, core in places])
    second = [(chip(z, y - 2, core), chip(z, y, core) + REACH) for z, y, core in places]
    return lax.ppermute(block, SP, [(a, b) for a, b in second if b < count])


def local(tokens, query_weight, key_weight, value_weight, out_weight):
    even = lax.axis_index("yc") % 2 == 0
    queries, near, far, pack = project(tokens, query_weight, key_weight, value_weight)
    four = behind(far, 4)
    eight = round_the_back(far)
    two = behind(pack, 2)
    six = behind(four, 2)
    sent = (jnp.where(even, pack, two), jnp.where(even, two[: 2 * TOK], four))
    odd_near = other_core(jnp.concatenate(sent, axis=0))
    partial = first(queries, near, pack, odd_near, two, four)
    odd_near, six, eight = lax.optimization_barrier((odd_near, six, eight))
    sent = (jnp.where(even, four, six), jnp.where(even, six, eight))
    odd_far = other_core(jnp.concatenate(sent, axis=0))
    merged, total_log, mix_weight = finish(
        lax.axis_size("tp"), out_weight, queries, odd_far, six, eight, *partial
    )
    heads = swap(merged, "tp")
    return mix(heads, mix_weight, total_log)


def solution(mesh):
    devices = mesh.devices
    planes = Mesh(devices.reshape(devices.shape[0] // PLANE, PLANE, devices.shape[1]), ("z", "yc", "tp"))
    sp = ("z", "yc")
    return jax.shard_map(
        local,
        mesh=planes,
        in_specs=(P(sp, None), P(None, "tp"), P(None, "tp"), P(None, "tp"), P(None, "tp")),
        out_specs=(P(sp, "tp"), P("tp", sp)),
        check_vma=False,
    )
```

time: 62.5 us -> 67.5 us (1.080)
  the two profiles are of different devices: /device:TPU:64 before, /device:TPU:536 now
where the time goes in v3:
time: 67.5 us; the launch traced here: 67.1 us
  waiting for transfers between devices  25.5 us (38%)
  starting transfers between devices  21.3 us (32%)
  blocking collectives  11.4 us (17%)
  Pallas kernels  8.02 us (12%)
  between operations  0.77 us (1%)
    all_to_all x1, blocking collectives, swap(): return lax.all_to_all(blocks, axis, split_axis=0, concat_axis=0, tiled=True)  11.4 us
    ppermute x3, waiting for transfers between devices, behind(): lax.ppermute(block, SP, [(i - distance, i) for i in range(distance, count)])  9.84 us
    ppermute x1, waiting for transfers between devices, round_the_back(): return lax.ppermute(block, SP, [(a, b) for a, b in second if b < count])  9.43 us
    ppermute x3, starting transfers between devices, behind(): lax.ppermute(block, SP, [(i - distance, i) for i in range(distance, count)])  9.32 us
    ppermute x1, waiting for transfers between devices, round_the_back(): lax.ppermute(block, SP, [(chip(z, y, core), chip(z, y - 2, core)) for z,...  6.21 us
    ppermute x1, starting transfers between devices, round_the_back(): lax.ppermute(block, SP, [(chip(z, y, core), chip(z, y - 2, core)) for z,...  5.11 us
    pallas_call x1, Pallas kernels, project(): pl.pallas_call(project_body, in_specs=[pl.BlockSpec(memory_space=pl.ANY)]...  3.91 us
    ppermute x2, starting transfers between devices, other_core(): lax.ppermute(block, SP, [(i, i ^ 1) for i in range(lax.axis_size(SP))])  3.84 us
  transfers between devices with their start and end apart: 7, of which 4 were waited for; matrix products, arithmetic and copies ran while one was open for 0% of the time, Pallas kernels for 3%

profile of v3, /device:TPU:536, one launch (start us, length us, event | category | flops | bytes accessed | tf_op | source)
XLA Modules:
  0.0 67.1 jit_solution(6185692882892980356)
XLA Ops:
  0.6 3.9 %project.1 = (bf16[3,256,128]{2,1,0:T(8,128)(2,1)S(1)}, bf16[2,128,128]{2,1,0:T(8,128)(2,1)S(1)}, bf16[512,128]{1,0:T(8,128)(2,1)S(1)}, bf16[1280,128]{1,0:T(8,128)(2,1)S(1)}) custom-call(bf16[256,2048]{1,0:T(8,128)(2,1)} %tok_hbm.1, bf16[2048,384]{1,0:T(8,128)(2,1)} %wq_hbm.1, bf16[2048,384]{1,0:T(8,128)(2,1)} %wk_hbm.1, bf16[2048,384]{1,0:T(8,128)(2,1)} %wv_hbm.1), custom_call_target="tpu_custom_call" | custom-call | tf_op jit(solution)/shard_map/project/pallas_call | solution.py:93
  4.6 4.7 %collective-permute-start.1 = (bf16[1280,128]{1,0:T(8,128)(2,1)S(1)}, bf16[1280,128]{1,0:T(8,128)(2,1)S(1)}, u32[]{:S(2)}, u32[]{:S(2)}) collective-permute-start(bf16[1280,128]{1,0:T(8,128)(2,1)S(1)} %get-tuple-element.16.own), channel_id=1, source_target_pairs={{0,8},{4,12},{8,16},{12,20},{16,24},{20,28},{24,32},{28,36},{32,40... | collective-permute-start | bytes 983048 | tf_op jit(solution)/shard_map/ppermute | solution.py:249
  9.3 2.7 %collective-permute-start = (bf16[512,128]{1,0:T(8,128)(2,1)S(1)}, bf16[512,128]{1,0:T(8,128)(2,1)S(1)}, u32[]{:S(2)}, u32[]{:S(2)}) collective-permute-start(bf16[512,128]{1,0:T(8,128)(2,1)S(1)} %get-tuple-element.15), channel_id=1, source_target_pairs={{0,16},{4,20},{8,24},{12,28},{16,32},{20,36},{24,40},{28,44},{32,4... | collective-permute-start | bytes 393224 | tf_op jit(solution)/shard_map/ppermute | solution.py:249
  12.0 7.9 %collective-permute-done.1.two = bf16[1280,128]{1,0:T(8,128)(2,1)S(1)} collective-permute-done((bf16[1280,128]{1,0:T(8,128)(2,1)S(1)}, bf16[1280,128]{1,0:T(8,128)(2,1)S(1)}, u32[]{:S(2)}, u32[]{:S(2)}) %collective-permute-start.1) | collective-permute-done | bytes 327712 | tf_op jit(solution)/shard_map/ppermute | solution.py:249
  19.9 2.0 %collective-permute-done.four = bf16[512,128]{1,0:T(8,128)(2,1)S(1)} collective-permute-done((bf16[512,128]{1,0:T(8,128)(2,1)S(1)}, bf16[512,128]{1,0:T(8,128)(2,1)S(1)}, u32[]{:S(2)}, u32[]{:S(2)}) %collective-permute-start) | collective-permute-done | bytes 131104 | tf_op jit(solution)/shard_map/ppermute | solution.py:249
  21.9 1.9 %collective-permute-start.2 = (bf16[1792,128]{1,0:T(8,128)(2,1)S(1)}, bf16[1792,128]{1,0:T(8,128)(2,1)S(1)}, u32[]{:S(2)}, u32[]{:S(2)}) collective-permute-start(bf16[1792,128]{1,0:T(8,128)(2,1)S(1)} %pad_maximum_fusion), channel_id=1, source_target_pairs={{0,4},{4,0},{8,12},{12,8},{16,20},{20,16},{24,28},{28,24},{32,36},... | collective-permute-start | bytes 1376264 | tf_op jit(solution)/shard_map/ppermute | solution.py:253
  23.8 5.1 %collective-permute-start.4 = (bf16[512,128]{1,0:T(8,128)(2,1)S(1)}, bf16[512,128]{1,0:T(8,128)(2,1)S(1)}, u32[]{:S(2)}, u32[]{:S(2)}) collective-permute-start(bf16[512,128]{1,0:T(8,128)(2,1)S(1)} %get-tuple-element.15), channel_id=1, source_target_pairs={{0,48},{4,52},{8,56},{12,60},{16,0},{20,4},{24,8},{28,12},{32,16},... | collective-permute-start | bytes 393224 | tf_op jit(solution)/shard_map/ppermute | solution.py:263
  29.0 1.9 %collective-permute-start.3 = (bf16[512,128]{1,0:T(8,128)(2,1)S(1)}, bf16[512,128]{1,0:T(8,128)(2,1)S(1)}, u32[]{:S(2)}, u32[]{:S(2)}) collective-permute-start(bf16[512,128]{1,0:T(8,128)(2,1)S(1)} %collective-permute-done.four), channel_id=1, source_target_pairs={{0,8},{4,12},{8,16},{12,20},{16,24},{20,28},{24,32},{28,36},{32,40... | collective-permute-start | bytes 393224 | tf_op jit(solution)/shard_map/ppermute | solution.py:249
  30.9 6.2 %collective-permute-done.4 = bf16[512,128]{1,0:T(8,128)(2,1)S(1)} collective-permute-done((bf16[512,128]{1,0:T(8,128)(2,1)S(1)}, bf16[512,128]{1,0:T(8,128)(2,1)S(1)}, u32[]{:S(2)}, u32[]{:S(2)}) %collective-permute-start.4) | collective-permute-done | bytes 131104 | tf_op jit(solution)/shard_map/ppermute | solution.py:263
  37.1 3.0 %collective-permute-start.5 = (bf16[512,128]{1,0:T(8,128)(2,1)S(1)}, bf16[512,128]{1,0:T(8,128)(2,1)S(1)}, u32[]{:S(2)}, u32[]{:S(2)}) collective-permute-start(bf16[512,128]{1,0:T(8,128)(2,1)S(1)} %collective-permute-done.4), channel_id=1, source_target_pairs={{48,32},{52,36},{56,40},{60,44},{0,48},{4,52},{8,56},{12,60},{16,6... | collective-permute-start | bytes 393224 | tf_op jit(solution)/shard_map/ppermute | solution.py:265
  40.2 0.0 collective-permute-done.3.six
  40.2 9.4 %collective-permute-done.5.eight = bf16[512,128]{1,0:T(8,128)(2,1)S(1)} collective-permute-done((bf16[512,128]{1,0:T(8,128)(2,1)S(1)}, bf16[512,128]{1,0:T(8,128)(2,1)S(1)}, u32[]{:S(2)}, u32[]{:S(2)}) %collective-permute-start.5) | collective-permute-done | bytes 131104 | tf_op jit(solution)/shard_map/ppermute | solution.py:265
  49.6 0.0 collective-permute-done.2.one
  49.7 1.9 %collective-permute-start.6 = (bf16[1024,128]{1,0:T(8,128)(2,1)S(1)}, bf16[1024,128]{1,0:T(8,128)(2,1)S(1)}, u32[]{:S(2)}, u32[]{:S(2)}) collective-permute-start(bf16[1024,128]{1,0:T(8,128)(2,1)S(1)} %pad_maximum_fusion.1), channel_id=1, source_target_pairs={{0,4},{4,0},{8,12},{12,8},{16,20},{20,16},{24,28},{28,24},{32,36},... | collective-permute-start | bytes 786440 | tf_op jit(solution)/shard_map/ppermute | solution.py:253
  51.6 1.9 %first.1 = (f32[256,128]{1,0:T(8,128)S(1)}, f32[256,128]{1,0:T(8,128)S(1)}, f32[256,128]{1,0:T(8,128)S(1)}) custom-call(bf16[3,256,128]{2,1,0:T(8,128)(2,1)S(1)} %get-tuple-element.14.queries, bf16[2,128,128]{2,1,0:T(8,128)(2,1)S(1)} %get-tuple-element.19.near, bf16[1280,128]{1,0:T(8,128)(2,1)S(1)} %get-tuple-element.16.own, ...), custom_call_target="tpu_custom_call" | custom-call | tf_op jit(solution)/shard_map/first/pallas_call | solution.py:179
  53.5 0.0 collective-permute-done.6.odd
  53.5 1.2 %finish.1 = (bf16[4,256,128]{2,1,0:T(8,128)(2,1)S(1)}, f32[1,256]{1,0:T(1,128)S(1)}, bf16[512,512]{1,0:T(8,128)(2,1)S(1)}) custom-call(bf16[3,256,128]{2,1,0:T(8,128)(2,1)S(1)} %get-tuple-element.14.queries, bf16[1024,128]{1,0:T(8,128)(2,1)S(1)} %collective-permute-done.6.odd, bf16[512,128]{1,0:T(8,128)(2,1)S(1)} %collective-permute-done.3.six, ...), custom_call_target="tpu_custom_call" | custom-call | tf_op jit(solution)/shard_map/finish/pallas_call | solution.py:214
  54.7 11.4 %all_to_all.5.heads = bf16[4,256,128]{2,1,0:T(8,128)(2,1)S(1)} all-to-all(bf16[4,256,128]{2,1,0:T(8,128)(2,1)S(1)} %get-tuple-element.23), channel_id=1, replica_groups=mesh['z'=16,'yc'=16,'tp'=4] {'tp'}, dimensions={0} | all-to-all | bytes 524288 | tf_op jit(solution)/shard_map/all_to_all | solution.py:241
  66.1 1.0 %mix.1 = (bf16[256,512]{1,0:T(8,128)(2,1)}, f32[1,256]{1,0:T(1,128)}) custom-call(bf16[4,256,128]{2,1,0:T(8,128)(2,1)S(1)} %all_to_all.5.heads, bf16[512,512]{1,0:T(8,128)(2,1)S(1)} %get-tuple-element.24.weight, f32[1,256]{1,0:T(1,128)S(1)} %get-tuple-element.25.log), custom_call_target="tpu_custom_call" | custom-call | tf_op jit(solution)/shard_map/mix/pallas_call | solution.py:231
  (5 shorter events, 0.1 us)
Async XLA Ops:
  4.6 15.3 %collective-permute-start.1 = (bf16[1280,128]{1,0:T(8,128)(2,1)S(1)}, bf16[1280,128]{1,0:T(8,128)(2,1)S(1)}, u32[]{:S(2)}, u32[]{:S(2)}) collective-permute-start(bf16[1280,128]{1,0:T(8,128)(2,1)S(1)} %get-tuple-element.16.own), channel_id=1, source_target_pairs={{0,8},{4,12},{8,16},{12,20},{16,24},{20,28},{24,32},{28,36},{32,40... | collective-permute-start | bytes 983048 | tf_op jit(solution)/shard_map/ppermute | solution.py:249
  9.3 12.6 %collective-permute-start = (bf16[512,128]{1,0:T(8,128)(2,1)S(1)}, bf16[512,128]{1,0:T(8,128)(2,1)S(1)}, u32[]{:S(2)}, u32[]{:S(2)}) collective-permute-start(bf16[512,128]{1,0:T(8,128)(2,1)S(1)} %get-tuple-element.15), channel_id=1, source_target_pairs={{0,16},{4,20},{8,24},{12,28},{16,32},{20,36},{24,40},{28,44},{32,4... | collective-permute-start | bytes 393224 | tf_op jit(solution)/shard_map/ppermute | solution.py:249
  21.9 27.7 %collective-permute-start.2 = (bf16[1792,128]{1,0:T(8,128)(2,1)S(1)}, bf16[1792,128]{1,0:T(8,128)(2,1)S(1)}, u32[]{:S(2)}, u32[]{:S(2)}) collective-permute-start(bf16[1792,128]{1,0:T(8,128)(2,1)S(1)} %pad_maximum_fusion), channel_id=1, source_target_pairs={{0,4},{4,0},{8,12},{12,8},{16,20},{20,16},{24,28},{28,24},{32,36},... | collective-permute-start | bytes 1376264 | tf_op jit(solution)/shard_map/ppermute | solution.py:253
  23.8 13.3 %collective-permute-start.4 = (bf16[512,128]{1,0:T(8,128)(2,1)S(1)}, bf16[512,128]{1,0:T(8,128)(2,1)S(1)}, u32[]{:S(2)}, u32[]{:S(2)}) collective-permute-start(bf16[512,128]{1,0:T(8,128)(2,1)S(1)} %get-tuple-element.15), channel_id=1, source_target_pairs={{0,48},{4,52},{8,56},{12,60},{16,0},{20,4},{24,8},{28,12},{32,16},... | collective-permute-start | bytes 393224 | tf_op jit(solution)/shard_map/ppermute | solution.py:263
  29.0 11.2 %collective-permute-start.3 = (bf16[512,128]{1,0:T(8,128)(2,1)S(1)}, bf16[512,128]{1,0:T(8,128)(2,1)S(1)}, u32[]{:S(2)}, u32[]{:S(2)}) collective-permute-start(bf16[512,128]{1,0:T(8,128)(2,1)S(1)} %collective-permute-done.four), channel_id=1, source_target_pairs={{0,8},{4,12},{8,16},{12,20},{16,24},{20,28},{24,32},{28,36},{32,40... | collective-permute-start | bytes 393224 | tf_op jit(solution)/shard_map/ppermute | solution.py:249
  37.1 12.5 %collective-permute-start.5 = (bf16[512,128]{1,0:T(8,128)(2,1)S(1)}, bf16[512,128]{1,0:T(8,128)(2,1)S(1)}, u32[]{:S(2)}, u32[]{:S(2)}) collective-permute-start(bf16[512,128]{1,0:T(8,128)(2,1)S(1)} %collective-permute-done.4), channel_id=1, source_target_pairs={{48,32},{52,36},{56,40},{60,44},{0,48},{4,52},{8,56},{12,60},{16,6... | collective-permute-start | bytes 393224 | tf_op jit(solution)/shard_map/ppermute | solution.py:265
  49.7 3.9 %collective-permute-start.6 = (bf16[1024,128]{1,0:T(8,128)(2,1)S(1)}, bf16[1024,128]{1,0:T(8,128)(2,1)S(1)}, u32[]{:S(2)}, u32[]{:S(2)}) collective-permute-start(bf16[1024,128]{1,0:T(8,128)(2,1)S(1)} %pad_maximum_fusion.1), channel_id=1, source_target_pairs={{0,4},{4,0},{8,12},{12,8},{16,20},{20,16},{24,28},{28,24},{32,36},... | collective-permute-start | bytes 786440 | tf_op jit(solution)/shard_map/ppermute | solution.py:253

commit v4 on v3

--- a/solution.py
+++ b/solution.py
@@ -14,6 +14,7 @@
 FAR_DILATION = 16
 REACH = 8
 SCALE = HEAD_DIM**-0.5
+PIECES = 2
 F32 = jnp.float32
 BF16 = jnp.bfloat16
 VMEM = pltpu.VMEM
@@ -56,36 +57,38 @@
 
 
 def project_body(tok_hbm, wq_hbm, wk_hbm, wv_hbm, queries, near, far, pack, tok, wq, wk, wv, sems):
-    pairs = ((tok_hbm, tok), (wk_hbm, wk), (wv_hbm, wv), (wq_hbm, wq))
-    copies = []
-    for j, (source, target) in enumerate(pairs):
-        half = source.shape[0] // 2
-        parts = [
-            pltpu.make_async_copy(source.at[pl.ds(i * half, half)], target.at[pl.ds(i * half, half)], sems.at[j, i])
-            for i in range(2)
-        ]
-        for part in parts:
-            part.start()
-        copies.append(parts)
-
-    def arrive(j):
-        for part in copies[j]:
-            part.wait()
-
     d = HEAD_DIM
-    arrive(0)
-    for j, weight in enumerate((wk, wv)):
-        arrive(j + 1)
-        rows = jnp.dot(tok[...], weight[...], preferred_element_type=F32).astype(BF16)
+    piece = tok.shape[1] // PIECES
+    spans = [pl.ds(i * piece, piece) for i in range(PIECES)]
+    tokens_in = [pltpu.make_async_copy(tok_hbm.at[:, span], tok.at[:, span], sems.at[3, i]) for i, span in enumerate(spans)]
+    weights_in = [
+        [pltpu.make_async_copy(source.at[span], target.at[span], sems.at[j, i]) for i, span in enumerate(spans)]
+        for j, (source, target) in enumerate(((wk_hbm, wk), (wv_hbm, wv), (wq_hbm, wq)))
+    ]
+    for i in range(PIECES):
+        tokens_in[i].start()
+        weights_in[0][i].start()
+    for part in weights_in[1] + weights_in[2]:
+        part.start()
+    for j, weight in enumerate((wk, wv, wq)):
+        total = None
+        for i in range(PIECES):
+            if j == 0:
+                tokens_in[i].wait()
+            weights_in[j][i].wait()
+            part = slice(i * piece, (i + 1) * piece)
+            product = jnp.dot(tok[:, part], weight[part], preferred_element_type=F32)
+            total = product if total is None else total + product
+        rows = total.astype(BF16)
+        if j == 2:
+            for group in range(3):
+                queries[group] = rows[:, group * d : (group + 1) * d]
+            break
         far[j * TOK : (j + 1) * TOK] = rows[:, 2 * d :]
         pack[j * TOK : (j + 1) * TOK] = rows[:, 2 * d :]
         pack[(2 + j) * TOK : (3 + j) * TOK] = rows[:, d : 2 * d]
         near[j] = rows[:BAND, :d]
         pack[4 * TOK + j * BAND : 4 * TOK + (j + 1) * BAND] = rows[BAND:, :d]
-    arrive(3)
-    rows = jnp.dot(tok[...], wq[...], preferred_element_type=F32).astype(BF16)
-    for j in range(3):
-        queries[j] = rows[:, j * d : (j + 1) * d]
 
 
 def project(tokens, wq, wk, wv):
@@ -100,7 +103,8 @@
             VMEM((2 * TOK, d), BF16),
             VMEM((4 * TOK + 2 * BAND, d), BF16),
         ],
-        scratch_shapes=[pltpu.VMEM(a.shape, a.dtype) for a in (tokens, wq, wk, wv)] + [pltpu.SemaphoreType.DMA((4, 2))],
+        scratch_shapes=[pltpu.VMEM(a.shape, a.dtype) for a in (tokens, wq, wk, wv)]
+        + [pltpu.SemaphoreType.DMA((4, PIECES))],
         name="project",
     )(*[pltpu.with_memory_space_constraint(a, pltpu.HBM) for a in (tokens, wq, wk, wv)])
 

time: 67.5 us -> 67.7 us (level)
  no operation moved by 1% of the time
where the time goes in v4:
time: 67.7 us; the launch traced here: 67.4 us
  waiting for transfers between devices  25.5 us (38%)
  starting transfers between devices  21.3 us (31%)
  blocking collectives  11.4 us (17%)
  Pallas kernels  8.23 us (12%)
  between operations  0.77 us (1%)
    all_to_all x1, blocking collectives, swap(): return lax.all_to_all(blocks, axis, split_axis=0, concat_axis=0, tiled=True)  11.4 us
    ppermute x3, waiting for transfers between devices, behind(): lax.ppermute(block, SP, [(i - distance, i) for i in range(distance, count)])  9.84 us
    ppermute x1, waiting for transfers between devices, round_the_back(): return lax.ppermute(block, SP, [(a, b) for a, b in second if b < count])  9.44 us
    ppermute x3, starting transfers between devices, behind(): lax.ppermute(block, SP, [(i - distance, i) for i in range(distance, count)])  9.32 us
    ppermute x1, waiting for transfers between devices, round_the_back(): lax.ppermute(block, SP, [(chip(z, y, core), chip(z, y - 2, core)) for z,...  6.22 us
    ppermute x1, starting transfers between devices, round_the_back(): lax.ppermute(block, SP, [(chip(z, y, core), chip(z, y - 2, core)) for z,...  5.11 us
    pallas_call x1, Pallas kernels, project(): pl.pallas_call(project_body, in_specs=[pl.BlockSpec(memory_space=pl.ANY)]...  4.15 us
    ppermute x2, starting transfers between devices, other_core(): lax.ppermute(block, SP, [(i, i ^ 1) for i in range(lax.axis_size(SP))])  3.84 us
  transfers between devices with their start and end apart: 7, of which 4 were waited for; matrix products, arithmetic and copies ran while one was open for 0% of the time, Pallas kernels for 3%

profile of v4, /device:TPU:536, one launch (start us, length us, event | category | flops | bytes accessed | tf_op | source)
XLA Modules:
  0.0 67.4 jit_solution(14831515831275751145)
XLA Ops:
  0.6 4.1 %project.1 = (bf16[3,256,128]{2,1,0:T(8,128)(2,1)S(1)}, bf16[2,128,128]{2,1,0:T(8,128)(2,1)S(1)}, bf16[512,128]{1,0:T(8,128)(2,1)S(1)}, bf16[1280,128]{1,0:T(8,128)(2,1)S(1)}) custom-call(bf16[256,2048]{1,0:T(8,128)(2,1)} %tok_hbm.1, bf16[2048,384]{1,0:T(8,128)(2,1)} %wq_hbm.1, bf16[2048,384]{1,0:T(8,128)(2,1)} %wk_hbm.1, bf16[2048,384]{1,0:T(8,128)(2,1)} %wv_hbm.1), custom_call_target="tpu_custom_call" | custom-call | tf_op jit(solution)/shard_map/project/pallas_call | solution.py:96
  4.8 4.7 %collective-permute-start.1 = (bf16[1280,128]{1,0:T(8,128)(2,1)S(1)}, bf16[1280,128]{1,0:T(8,128)(2,1)S(1)}, u32[]{:S(2)}, u32[]{:S(2)}) collective-permute-start(bf16[1280,128]{1,0:T(8,128)(2,1)S(1)} %get-tuple-element.16.own), channel_id=1, source_target_pairs={{0,8},{4,12},{8,16},{12,20},{16,24},{20,28},{24,32},{28,36},{32,40... | collective-permute-start | bytes 983048 | tf_op jit(solution)/shard_map/ppermute | solution.py:253
  9.5 2.7 %collective-permute-start = (bf16[512,128]{1,0:T(8,128)(2,1)S(1)}, bf16[512,128]{1,0:T(8,128)(2,1)S(1)}, u32[]{:S(2)}, u32[]{:S(2)}) collective-permute-start(bf16[512,128]{1,0:T(8,128)(2,1)S(1)} %get-tuple-element.15), channel_id=1, source_target_pairs={{0,16},{4,20},{8,24},{12,28},{16,32},{20,36},{24,40},{28,44},{32,4... | collective-permute-start | bytes 393224 | tf_op jit(solution)/shard_map/ppermute | solution.py:253
  12.2 7.9 %collective-permute-done.1.two = bf16[1280,128]{1,0:T(8,128)(2,1)S(1)} collective-permute-done((bf16[1280,128]{1,0:T(8,128)(2,1)S(1)}, bf16[1280,128]{1,0:T(8,128)(2,1)S(1)}, u32[]{:S(2)}, u32[]{:S(2)}) %collective-permute-start.1) | collective-permute-done | bytes 327712 | tf_op jit(solution)/shard_map/ppermute | solution.py:253
  20.1 2.0 %collective-permute-done.four = bf16[512,128]{1,0:T(8,128)(2,1)S(1)} collective-permute-done((bf16[512,128]{1,0:T(8,128)(2,1)S(1)}, bf16[512,128]{1,0:T(8,128)(2,1)S(1)}, u32[]{:S(2)}, u32[]{:S(2)}) %collective-permute-start) | collective-permute-done | bytes 131104 | tf_op jit(solution)/shard_map/ppermute | solution.py:253
  22.1 1.9 %collective-permute-start.2 = (bf16[1792,128]{1,0:T(8,128)(2,1)S(1)}, bf16[1792,128]{1,0:T(8,128)(2,1)S(1)}, u32[]{:S(2)}, u32[]{:S(2)}) collective-permute-start(bf16[1792,128]{1,0:T(8,128)(2,1)S(1)} %pad_maximum_fusion), channel_id=1, source_target_pairs={{0,4},{4,0},{8,12},{12,8},{16,20},{20,16},{24,28},{28,24},{32,36},... | collective-permute-start | bytes 1376264 | tf_op jit(solution)/shard_map/ppermute | solution.py:257
  24.1 5.1 %collective-permute-start.4 = (bf16[512,128]{1,0:T(8,128)(2,1)S(1)}, bf16[512,128]{1,0:T(8,128)(2,1)S(1)}, u32[]{:S(2)}, u32[]{:S(2)}) collective-permute-start(bf16[512,128]{1,0:T(8,128)(2,1)S(1)} %get-tuple-element.15), channel_id=1, source_target_pairs={{0,48},{4,52},{8,56},{12,60},{16,0},{20,4},{24,8},{28,12},{32,16},... | collective-permute-start | bytes 393224 | tf_op jit(solution)/shard_map/ppermute | solution.py:267
  29.2 1.9 %collective-permute-start.3 = (bf16[512,128]{1,0:T(8,128)(2,1)S(1)}, bf16[512,128]{1,0:T(8,128)(2,1)S(1)}, u32[]{:S(2)}, u32[]{:S(2)}) collective-permute-start(bf16[512,128]{1,0:T(8,128)(2,1)S(1)} %collective-permute-done.four), channel_id=1, source_target_pairs={{0,8},{4,12},{8,16},{12,20},{16,24},{20,28},{24,32},{28,36},{32,40... | collective-permute-start | bytes 393224 | tf_op jit(solution)/shard_map/ppermute | solution.py:253
  31.1 6.2 %collective-permute-done.4 = bf16[512,128]{1,0:T(8,128)(2,1)S(1)} collective-permute-done((bf16[512,128]{1,0:T(8,128)(2,1)S(1)}, bf16[512,128]{1,0:T(8,128)(2,1)S(1)}, u32[]{:S(2)}, u32[]{:S(2)}) %collective-permute-start.4) | collective-permute-done | bytes 131104 | tf_op jit(solution)/shard_map/ppermute | solution.py:267
  37.3 3.0 %collective-permute-start.5 = (bf16[512,128]{1,0:T(8,128)(2,1)S(1)}, bf16[512,128]{1,0:T(8,128)(2,1)S(1)}, u32[]{:S(2)}, u32[]{:S(2)}) collective-permute-start(bf16[512,128]{1,0:T(8,128)(2,1)S(1)} %collective-permute-done.4), channel_id=1, source_target_pairs={{48,32},{52,36},{56,40},{60,44},{0,48},{4,52},{8,56},{12,60},{16,6... | collective-permute-start | bytes 393224 | tf_op jit(solution)/shard_map/ppermute | solution.py:269
  40.4 0.0 collective-permute-done.3.six
  40.4 9.4 %collective-permute-done.5.eight = bf16[512,128]{1,0:T(8,128)(2,1)S(1)} collective-permute-done((bf16[512,128]{1,0:T(8,128)(2,1)S(1)}, bf16[512,128]{1,0:T(8,128)(2,1)S(1)}, u32[]{:S(2)}, u32[]{:S(2)}) %collective-permute-start.5) | collective-permute-done | bytes 131104 | tf_op jit(solution)/shard_map/ppermute | solution.py:269
  49.8 0.0 collective-permute-done.2.one
  49.9 1.9 %collective-permute-start.6 = (bf16[1024,128]{1,0:T(8,128)(2,1)S(1)}, bf16[1024,128]{1,0:T(8,128)(2,1)S(1)}, u32[]{:S(2)}, u32[]{:S(2)}) collective-permute-start(bf16[1024,128]{1,0:T(8,128)(2,1)S(1)} %pad_maximum_fusion.1), channel_id=1, source_target_pairs={{0,4},{4,0},{8,12},{12,8},{16,20},{20,16},{24,28},{28,24},{32,36},... | collective-permute-start | bytes 786440 | tf_op jit(solution)/shard_map/ppermute | solution.py:257
  51.8 1.9 %first.1 = (f32[256,128]{1,0:T(8,128)S(1)}, f32[256,128]{1,0:T(8,128)S(1)}, f32[256,128]{1,0:T(8,128)S(1)}) custom-call(bf16[3,256,128]{2,1,0:T(8,128)(2,1)S(1)} %get-tuple-element.14.queries, bf16[2,128,128]{2,1,0:T(8,128)(2,1)S(1)} %get-tuple-element.19.near, bf16[1280,128]{1,0:T(8,128)(2,1)S(1)} %get-tuple-element.16.own, ...), custom_call_target="tpu_custom_call" | custom-call | tf_op jit(solution)/shard_map/first/pallas_call | solution.py:183
  53.8 0.0 collective-permute-done.6.odd
  53.8 1.1 %finish.1 = (bf16[4,256,128]{2,1,0:T(8,128)(2,1)S(1)}, f32[1,256]{1,0:T(1,128)S(1)}, bf16[512,512]{1,0:T(8,128)(2,1)S(1)}) custom-call(bf16[3,256,128]{2,1,0:T(8,128)(2,1)S(1)} %get-tuple-element.14.queries, bf16[1024,128]{1,0:T(8,128)(2,1)S(1)} %collective-permute-done.6.odd, bf16[512,128]{1,0:T(8,128)(2,1)S(1)} %collective-permute-done.3.six, ...), custom_call_target="tpu_custom_call" | custom-call | tf_op jit(solution)/shard_map/finish/pallas_call | solution.py:218
  54.9 11.4 %all_to_all.5.heads = bf16[4,256,128]{2,1,0:T(8,128)(2,1)S(1)} all-to-all(bf16[4,256,128]{2,1,0:T(8,128)(2,1)S(1)} %get-tuple-element.23), channel_id=1, replica_groups=mesh['z'=16,'yc'=16,'tp'=4] {'tp'}, dimensions={0} | all-to-all | bytes 524288 | tf_op jit(solution)/shard_map/all_to_all | solution.py:245
  66.4 1.0 %mix.1 = (bf16[256,512]{1,0:T(8,128)(2,1)}, f32[1,256]{1,0:T(1,128)}) custom-call(bf16[4,256,128]{2,1,0:T(8,128)(2,1)S(1)} %all_to_all.5.heads, bf16[512,512]{1,0:T(8,128)(2,1)S(1)} %get-tuple-element.24.weight, f32[1,256]{1,0:T(1,128)S(1)} %get-tuple-element.25.log), custom_call_target="tpu_custom_call" | custom-call | tf_op jit(solution)/shard_map/mix/pallas_call | solution.py:235
  (5 shorter events, 0.1 us)
Async XLA Ops:
  4.8 15.3 %collective-permute-start.1 = (bf16[1280,128]{1,0:T(8,128)(2,1)S(1)}, bf16[1280,128]{1,0:T(8,128)(2,1)S(1)}, u32[]{:S(2)}, u32[]{:S(2)}) collective-permute-start(bf16[1280,128]{1,0:T(8,128)(2,1)S(1)} %get-tuple-element.16.own), channel_id=1, source_target_pairs={{0,8},{4,12},{8,16},{12,20},{16,24},{20,28},{24,32},{28,36},{32,40... | collective-permute-start | bytes 983048 | tf_op jit(solution)/shard_map/ppermute | solution.py:253
  9.5 12.6 %collective-permute-start = (bf16[512,128]{1,0:T(8,128)(2,1)S(1)}, bf16[512,128]{1,0:T(8,128)(2,1)S(1)}, u32[]{:S(2)}, u32[]{:S(2)}) collective-permute-start(bf16[512,128]{1,0:T(8,128)(2,1)S(1)} %get-tuple-element.15), channel_id=1, source_target_pairs={{0,16},{4,20},{8,24},{12,28},{16,32},{20,36},{24,40},{28,44},{32,4... | collective-permute-start | bytes 393224 | tf_op jit(solution)/shard_map/ppermute | solution.py:253
  22.1 27.7 %collective-permute-start.2 = (bf16[1792,128]{1,0:T(8,128)(2,1)S(1)}, bf16[1792,128]{1,0:T(8,128)(2,1)S(1)}, u32[]{:S(2)}, u32[]{:S(2)}) collective-permute-start(bf16[1792,128]{1,0:T(8,128)(2,1)S(1)} %pad_maximum_fusion), channel_id=1, source_target_pairs={{0,4},{4,0},{8,12},{12,8},{16,20},{20,16},{24,28},{28,24},{32,36},... | collective-permute-start | bytes 1376264 | tf_op jit(solution)/shard_map/ppermute | solution.py:257
  24.1 13.3 %collective-permute-start.4 = (bf16[512,128]{1,0:T(8,128)(2,1)S(1)}, bf16[512,128]{1,0:T(8,128)(2,1)S(1)}, u32[]{:S(2)}, u32[]{:S(2)}) collective-permute-start(bf16[512,128]{1,0:T(8,128)(2,1)S(1)} %get-tuple-element.15), channel_id=1, source_target_pairs={{0,48},{4,52},{8,56},{12,60},{16,0},{20,4},{24,8},{28,12},{32,16},... | collective-permute-start | bytes 393224 | tf_op jit(solution)/shard_map/ppermute | solution.py:267
  29.2 11.2 %collective-permute-start.3 = (bf16[512,128]{1,0:T(8,128)(2,1)S(1)}, bf16[512,128]{1,0:T(8,128)(2,1)S(1)}, u32[]{:S(2)}, u32[]{:S(2)}) collective-permute-start(bf16[512,128]{1,0:T(8,128)(2,1)S(1)} %collective-permute-done.four), channel_id=1, source_target_pairs={{0,8},{4,12},{8,16},{12,20},{16,24},{20,28},{24,32},{28,36},{32,40... | collective-permute-start | bytes 393224 | tf_op jit(solution)/shard_map/ppermute | solution.py:253
  37.3 12.5 %collective-permute-start.5 = (bf16[512,128]{1,0:T(8,128)(2,1)S(1)}, bf16[512,128]{1,0:T(8,128)(2,1)S(1)}, u32[]{:S(2)}, u32[]{:S(2)}) collective-permute-start(bf16[512,128]{1,0:T(8,128)(2,1)S(1)} %collective-permute-done.4), channel_id=1, source_target_pairs={{48,32},{52,36},{56,40},{60,44},{0,48},{4,52},{8,56},{12,60},{16,6... | collective-permute-start | bytes 393224 | tf_op jit(solution)/shard_map/ppermute | solution.py:269
  49.9 3.9 %collective-permute-start.6 = (bf16[1024,128]{1,0:T(8,128)(2,1)S(1)}, bf16[1024,128]{1,0:T(8,128)(2,1)S(1)}, u32[]{:S(2)}, u32[]{:S(2)}) collective-permute-start(bf16[1024,128]{1,0:T(8,128)(2,1)S(1)} %pad_maximum_fusion.1), channel_id=1, source_target_pairs={{0,4},{4,0},{8,12},{12,8},{16,20},{20,16},{24,28},{28,24},{32,36},... | collective-permute-start | bytes 786440 | tf_op jit(solution)/shard_map/ppermute | solution.py:257

commit v5 on v3

--- a/solution.py
+++ b/solution.py
@@ -140,7 +140,24 @@
     return lax.axis_index("z") * PLANE + lax.axis_index("yc")
 
 
-def first_body(queries, near, own, one, two, four, attended, far_rows, stats):
+def early_body(queries, own, two, four, far_rows, stats):
+    blocks = ((0, own, 0), (2, two, 0), (4, four, 0))
+    highest, total, rows = Far(queries[2], head_slope(), place_here()).gather(blocks)
+    far_rows[...] = rows
+    stats[...] = jnp.where(iota(stats.shape, 1) == 0, highest, total)
+
+
+def early(*arrays):
+    return pl.pallas_call(
+        early_body,
+        in_specs=[WHOLE] * len(arrays),
+        out_specs=[WHOLE] * 2,
+        out_shape=[VMEM((TOK, HEAD_DIM), F32)] * 2,
+        name="early",
+    )(*held(*arrays))
+
+
+def first_body(queries, near, own, one, two, early_rows, early_stats, attended, far_rows, stats):
     slope = head_slope()
     place = place_here()
     b, at = BAND, 4 * TOK
@@ -167,9 +184,12 @@
     attended[...] = (first_share * inverse) * first + (second_share * inverse) * second
     log = highest + jnp.log(total)
 
-    blocks = ((0, own, 0), (1, one, 0), (2, two, 0), (3, one, 4 * TOK + 2 * BAND), (4, four, 0))
-    highest, total, rows = Far(queries[2], slope, place).gather(blocks)
-    far_rows[...] = rows
+    blocks = ((1, one, 0), (3, one, 4 * TOK + 2 * BAND))
+    before = early_stats[:, 0:1]
+    highest, total, rows = Far(queries[2], slope, place).gather(blocks, before)
+    kept = jnp.exp(before - highest)
+    total = total + kept * early_stats[:, 1:2]
+    far_rows[...] = rows + kept * early_rows[...]
     lanes = iota(stats.shape, 1)
     stats[...] = jnp.where(lanes == 0, log, jnp.where(lanes == 1, highest, total))
 
@@ -274,7 +294,8 @@
     six = behind(four, 2)
     sent = (jnp.where(even, pack, two), jnp.where(even, two[: 2 * TOK], four))
     odd_near = other_core(jnp.concatenate(sent, axis=0))
-    partial = first(queries, near, pack, odd_near, two, four)
+    begun = early(queries, pack, two, four)
+    partial = first(queries, near, pack, odd_near, two, *begun)
     odd_near, six, eight = lax.optimization_barrier((odd_near, six, eight))
     sent = (jnp.where(even, four, six), jnp.where(even, six, eight))
     odd_far = other_core(jnp.concatenate(sent, axis=0))

time: 67.5 us -> 68 us (level)
  the two profiles are of different devices: /device:TPU:536 before, /device:TPU:280 now
where the time goes in v5:
time: 68 us; the launch traced here: 67.6 us
  waiting for transfers between devices  24.6 us (36%)
  starting transfers between devices  22.2 us (33%)
  blocking collectives  11.4 us (17%)
  Pallas kernels  8.47 us (12%)
  between operations  0.77 us (1%)
    all_to_all x1, blocking collectives, swap(): return lax.all_to_all(blocks, axis, split_axis=0, concat_axis=0, tiled=True)  11.4 us
    ppermute x3, waiting for transfers between devices, behind(): lax.ppermute(block, SP, [(i - distance, i) for i in range(distance, count)])  9.84 us
    ppermute x3, starting transfers between devices, behind(): lax.ppermute(block, SP, [(i - distance, i) for i in range(distance, count)])  9.32 us
    ppermute x1, waiting for transfers between devices, round_the_back(): return lax.ppermute(block, SP, [(a, b) for a, b in second if b < count])  8.54 us
    ppermute x1, waiting for transfers between devices, round_the_back(): lax.ppermute(block, SP, [(chip(z, y, core), chip(z, y - 2, core)) for z,...  6.21 us
    ppermute x1, starting transfers between devices, round_the_back(): lax.ppermute(block, SP, [(chip(z, y, core), chip(z, y - 2, core)) for z,...  5.12 us
    ppermute x1, starting transfers between devices, round_the_back(): return lax.ppermute(block, SP, [(a, b) for a, b in second if b < count])  3.94 us
    pallas_call x1, Pallas kernels, project(): pl.pallas_call(project_body, in_specs=[pl.BlockSpec(memory_space=pl.ANY)]...  3.92 us
  transfers between devices with their start and end apart: 7, of which 4 were waited for; matrix products, arithmetic and copies ran while one was open for 0% of the time, Pallas kernels for 4%

profile of v5, /device:TPU:280, one launch (start us, length us, event | category | flops | bytes accessed | tf_op | source)
XLA Modules:
  0.0 67.6 jit_solution(4528980589281494024)
XLA Ops:
  0.6 3.9 %project.1 = (bf16[3,256,128]{2,1,0:T(8,128)(2,1)S(1)}, bf16[2,128,128]{2,1,0:T(8,128)(2,1)S(1)}, bf16[512,128]{1,0:T(8,128)(2,1)S(1)}, bf16[1280,128]{1,0:T(8,128)(2,1)S(1)}) custom-call(bf16[256,2048]{1,0:T(8,128)(2,1)} %tok_hbm.1, bf16[2048,384]{1,0:T(8,128)(2,1)} %wq_hbm.1, bf16[2048,384]{1,0:T(8,128)(2,1)} %wk_hbm.1, bf16[2048,384]{1,0:T(8,128)(2,1)} %wv_hbm.1), custom_call_target="tpu_custom_call" | custom-call | tf_op jit(solution)/shard_map/project/pallas_call | solution.py:93
  4.6 4.7 %collective-permute-start.1 = (bf16[1280,128]{1,0:T(8,128)(2,1)S(1)}, bf16[1280,128]{1,0:T(8,128)(2,1)S(1)}, u32[]{:S(2)}, u32[]{:S(2)}) collective-permute-start(bf16[1280,128]{1,0:T(8,128)(2,1)S(1)} %get-tuple-element.18.own), channel_id=1, source_target_pairs={{0,8},{4,12},{8,16},{12,20},{16,24},{20,28},{24,32},{28,36},{32,40... | collective-permute-start | bytes 983048 | tf_op jit(solution)/shard_map/ppermute | solution.py:269
  9.3 2.7 %collective-permute-start = (bf16[512,128]{1,0:T(8,128)(2,1)S(1)}, bf16[512,128]{1,0:T(8,128)(2,1)S(1)}, u32[]{:S(2)}, u32[]{:S(2)}) collective-permute-start(bf16[512,128]{1,0:T(8,128)(2,1)S(1)} %get-tuple-element.17), channel_id=1, source_target_pairs={{0,16},{4,20},{8,24},{12,28},{16,32},{20,36},{24,40},{28,44},{32,4... | collective-permute-start | bytes 393224 | tf_op jit(solution)/shard_map/ppermute | solution.py:269
  12.0 7.9 %collective-permute-done.1.two = bf16[1280,128]{1,0:T(8,128)(2,1)S(1)} collective-permute-done((bf16[1280,128]{1,0:T(8,128)(2,1)S(1)}, bf16[1280,128]{1,0:T(8,128)(2,1)S(1)}, u32[]{:S(2)}, u32[]{:S(2)}) %collective-permute-start.1) | collective-permute-done | bytes 327712 | tf_op jit(solution)/shard_map/ppermute | solution.py:269
  19.9 2.0 %collective-permute-done.four = bf16[512,128]{1,0:T(8,128)(2,1)S(1)} collective-permute-done((bf16[512,128]{1,0:T(8,128)(2,1)S(1)}, bf16[512,128]{1,0:T(8,128)(2,1)S(1)}, u32[]{:S(2)}, u32[]{:S(2)}) %collective-permute-start) | collective-permute-done | bytes 131104 | tf_op jit(solution)/shard_map/ppermute | solution.py:269
  21.9 1.9 %collective-permute-start.2 = (bf16[1792,128]{1,0:T(8,128)(2,1)S(1)}, bf16[1792,128]{1,0:T(8,128)(2,1)S(1)}, u32[]{:S(2)}, u32[]{:S(2)}) collective-permute-start(bf16[1792,128]{1,0:T(8,128)(2,1)S(1)} %pad_maximum_fusion), channel_id=1, source_target_pairs={{0,4},{4,0},{8,12},{12,8},{16,20},{20,16},{24,28},{28,24},{32,36},... | collective-permute-start | bytes 1376264 | tf_op jit(solution)/shard_map/ppermute | solution.py:273
  23.8 5.1 %collective-permute-start.4 = (bf16[512,128]{1,0:T(8,128)(2,1)S(1)}, bf16[512,128]{1,0:T(8,128)(2,1)S(1)}, u32[]{:S(2)}, u32[]{:S(2)}) collective-permute-start(bf16[512,128]{1,0:T(8,128)(2,1)S(1)} %get-tuple-element.17), channel_id=1, source_target_pairs={{0,48},{4,52},{8,56},{12,60},{16,0},{20,4},{24,8},{28,12},{32,16},... | collective-permute-start | bytes 393224 | tf_op jit(solution)/shard_map/ppermute | solution.py:283
  29.0 1.9 %collective-permute-start.3 = (bf16[512,128]{1,0:T(8,128)(2,1)S(1)}, bf16[512,128]{1,0:T(8,128)(2,1)S(1)}, u32[]{:S(2)}, u32[]{:S(2)}) collective-permute-start(bf16[512,128]{1,0:T(8,128)(2,1)S(1)} %collective-permute-done.four), channel_id=1, source_target_pairs={{0,8},{4,12},{8,16},{12,20},{16,24},{20,28},{24,32},{28,36},{32,40... | collective-permute-start | bytes 393224 | tf_op jit(solution)/shard_map/ppermute | solution.py:269
  30.9 6.2 %collective-permute-done.4 = bf16[512,128]{1,0:T(8,128)(2,1)S(1)} collective-permute-done((bf16[512,128]{1,0:T(8,128)(2,1)S(1)}, bf16[512,128]{1,0:T(8,128)(2,1)S(1)}, u32[]{:S(2)}, u32[]{:S(2)}) %collective-permute-start.4) | collective-permute-done | bytes 131104 | tf_op jit(solution)/shard_map/ppermute | solution.py:283
  37.1 3.9 %collective-permute-start.5 = (bf16[512,128]{1,0:T(8,128)(2,1)S(1)}, bf16[512,128]{1,0:T(8,128)(2,1)S(1)}, u32[]{:S(2)}, u32[]{:S(2)}) collective-permute-start(bf16[512,128]{1,0:T(8,128)(2,1)S(1)} %collective-permute-done.4), channel_id=1, source_target_pairs={{48,32},{52,36},{56,40},{60,44},{0,48},{4,52},{8,56},{12,60},{16,6... | collective-permute-start | bytes 393224 | tf_op jit(solution)/shard_map/ppermute | solution.py:285
  41.0 0.0 collective-permute-done.3.six
  41.1 8.5 %collective-permute-done.5.eight = bf16[512,128]{1,0:T(8,128)(2,1)S(1)} collective-permute-done((bf16[512,128]{1,0:T(8,128)(2,1)S(1)}, bf16[512,128]{1,0:T(8,128)(2,1)S(1)}, u32[]{:S(2)}, u32[]{:S(2)}) %collective-permute-start.5) | collective-permute-done | bytes 131104 | tf_op jit(solution)/shard_map/ppermute | solution.py:285
  49.6 0.0 collective-permute-done.2.one
  49.7 1.9 %collective-permute-start.6 = (bf16[1024,128]{1,0:T(8,128)(2,1)S(1)}, bf16[1024,128]{1,0:T(8,128)(2,1)S(1)}, u32[]{:S(2)}, u32[]{:S(2)}) collective-permute-start(bf16[1024,128]{1,0:T(8,128)(2,1)S(1)} %pad_maximum_fusion.1), channel_id=1, source_target_pairs={{0,4},{4,0},{8,12},{12,8},{16,20},{20,16},{24,28},{28,24},{32,36},... | collective-permute-start | bytes 786440 | tf_op jit(solution)/shard_map/ppermute | solution.py:273
  51.6 0.6 early.1
  52.2 1.8 %first.1 = (f32[256,128]{1,0:T(8,128)S(1)}, f32[256,128]{1,0:T(8,128)S(1)}, f32[256,128]{1,0:T(8,128)S(1)}) custom-call(bf16[3,256,128]{2,1,0:T(8,128)(2,1)S(1)} %get-tuple-element.16.queries, bf16[2,128,128]{2,1,0:T(8,128)(2,1)S(1)} %get-tuple-element.21.near, bf16[1280,128]{1,0:T(8,128)(2,1)S(1)} %get-tuple-element.18.own, ...), custom_call_target="tpu_custom_call" | custom-call | tf_op jit(solution)/shard_map/first/pallas_call | solution.py:199
  54.0 0.0 collective-permute-done.6.odd
  54.0 1.1 %finish.1 = (bf16[4,256,128]{2,1,0:T(8,128)(2,1)S(1)}, f32[1,256]{1,0:T(1,128)S(1)}, bf16[512,512]{1,0:T(8,128)(2,1)S(1)}) custom-call(bf16[3,256,128]{2,1,0:T(8,128)(2,1)S(1)} %get-tuple-element.16.queries, bf16[1024,128]{1,0:T(8,128)(2,1)S(1)} %collective-permute-done.6.odd, bf16[512,128]{1,0:T(8,128)(2,1)S(1)} %collective-permute-done.3.six, ...), custom_call_target="tpu_custom_call" | custom-call | tf_op jit(solution)/shard_map/finish/pallas_call | solution.py:234
  55.2 11.4 %all_to_all.5.heads = bf16[4,256,128]{2,1,0:T(8,128)(2,1)S(1)} all-to-all(bf16[4,256,128]{2,1,0:T(8,128)(2,1)S(1)} %get-tuple-element.27), channel_id=1, replica_groups=mesh['z'=16,'yc'=16,'tp'=4] {'tp'}, dimensions={0} | all-to-all | bytes 524288 | tf_op jit(solution)/shard_map/all_to_all | solution.py:261
  66.6 1.0 %mix.1 = (bf16[256,512]{1,0:T(8,128)(2,1)}, f32[1,256]{1,0:T(1,128)}) custom-call(bf16[4,256,128]{2,1,0:T(8,128)(2,1)S(1)} %all_to_all.5.heads, bf16[512,512]{1,0:T(8,128)(2,1)S(1)} %get-tuple-element.28.weight, f32[1,256]{1,0:T(1,128)S(1)} %get-tuple-element.29.log), custom_call_target="tpu_custom_call" | custom-call | tf_op jit(solution)/shard_map/mix/pallas_call | solution.py:251
  (5 shorter events, 0.1 us)
Async XLA Ops:
  4.6 15.3 %collective-permute-start.1 = (bf16[1280,128]{1,0:T(8,128)(2,1)S(1)}, bf16[1280,128]{1,0:T(8,128)(2,1)S(1)}, u32[]{:S(2)}, u32[]{:S(2)}) collective-permute-start(bf16[1280,128]{1,0:T(8,128)(2,1)S(1)} %get-tuple-element.18.own), channel_id=1, source_target_pairs={{0,8},{4,12},{8,16},{12,20},{16,24},{20,28},{24,32},{28,36},{32,40... | collective-permute-start | bytes 983048 | tf_op jit(solution)/shard_map/ppermute | solution.py:269
  9.3 12.6 %collective-permute-start = (bf16[512,128]{1,0:T(8,128)(2,1)S(1)}, bf16[512,128]{1,0:T(8,128)(2,1)S(1)}, u32[]{:S(2)}, u32[]{:S(2)}) collective-permute-start(bf16[512,128]{1,0:T(8,128)(2,1)S(1)} %get-tuple-element.17), channel_id=1, source_target_pairs={{0,16},{4,20},{8,24},{12,28},{16,32},{20,36},{24,40},{28,44},{32,4... | collective-permute-start | bytes 393224 | tf_op jit(solution)/shard_map/ppermute | solution.py:269
  21.9 27.7 %collective-permute-start.2 = (bf16[1792,128]{1,0:T(8,128)(2,1)S(1)}, bf16[1792,128]{1,0:T(8,128)(2,1)S(1)}, u32[]{:S(2)}, u32[]{:S(2)}) collective-permute-start(bf16[1792,128]{1,0:T(8,128)(2,1)S(1)} %pad_maximum_fusion), channel_id=1, source_target_pairs={{0,4},{4,0},{8,12},{12,8},{16,20},{20,16},{24,28},{28,24},{32,36},... | collective-permute-start | bytes 1376264 | tf_op jit(solution)/shard_map/ppermute | solution.py:273
  23.8 13.3 %collective-permute-start.4 = (bf16[512,128]{1,0:T(8,128)(2,1)S(1)}, bf16[512,128]{1,0:T(8,128)(2,1)S(1)}, u32[]{:S(2)}, u32[]{:S(2)}) collective-permute-start(bf16[512,128]{1,0:T(8,128)(2,1)S(1)} %get-tuple-element.17), channel_id=1, source_target_pairs={{0,48},{4,52},{8,56},{12,60},{16,0},{20,4},{24,8},{28,12},{32,16},... | collective-permute-start | bytes 393224 | tf_op jit(solution)/shard_map/ppermute | solution.py:283
  29.0 12.1 %collective-permute-start.3 = (bf16[512,128]{1,0:T(8,128)(2,1)S(1)}, bf16[512,128]{1,0:T(8,128)(2,1)S(1)}, u32[]{:S(2)}, u32[]{:S(2)}) collective-permute-start(bf16[512,128]{1,0:T(8,128)(2,1)S(1)} %collective-permute-done.four), channel_id=1, source_target_pairs={{0,8},{4,12},{8,16},{12,20},{16,24},{20,28},{24,32},{28,36},{32,40... | collective-permute-start | bytes 393224 | tf_op jit(solution)/shard_map/ppermute | solution.py:269
  37.1 12.5 %collective-permute-start.5 = (bf16[512,128]{1,0:T(8,128)(2,1)S(1)}, bf16[512,128]{1,0:T(8,128)(2,1)S(1)}, u32[]{:S(2)}, u32[]{:S(2)}) collective-permute-start(bf16[512,128]{1,0:T(8,128)(2,1)S(1)} %collective-permute-done.4), channel_id=1, source_target_pairs={{48,32},{52,36},{56,40},{60,44},{0,48},{4,52},{8,56},{12,60},{16,6... | collective-permute-start | bytes 393224 | tf_op jit(solution)/shard_map/ppermute | solution.py:285
  49.7 4.4 %collective-permute-start.6 = (bf16[1024,128]{1,0:T(8,128)(2,1)S(1)}, bf16[1024,128]{1,0:T(8,128)(2,1)S(1)}, u32[]{:S(2)}, u32[]{:S(2)}) collective-permute-start(bf16[1024,128]{1,0:T(8,128)(2,1)S(1)} %pad_maximum_fusion.1), channel_id=1, source_target_pairs={{0,4},{4,0},{8,12},{12,8},{16,20},{20,16},{24,28},{28,24},{32,36},... | collective-permute-start | bytes 786440 | tf_op jit(solution)/shard_map/ppermute | solution.py:273
